TPU v7x, 32 devices: a whole 2x2x4 slice. The times are simulated.
32 devices in a mesh: sp: 8 (over z, x), tp: 4 (over y, core).
Axes of the slice: x: 2, y: 2, z: 4, core: 2. Of those that a mesh axis runs over, the one named last changes fastest.
Arguments:
- resid: bfloat16 [4096, 2048], P(('sp', 'tp')), may hold values from -6 to 6
- recurrent_input: bfloat16 [4096, 2048], P('sp', 'tp'), may hold values from -12.2 to 12.2
- recurrent_out_gate: bfloat16 [4096, 2048], P('sp', 'tp'), may hold values from -6 to 6
- filter_weight: float32 [4, 2048], P(None, 'tp'), may hold values from -3 to 3
- recurrence_gate_matrix: bfloat16 [32, 64, 64], P('tp'), may hold values from -0.75 to 0.75
- input_gate_matrix: bfloat16 [32, 64, 64], P('tp'), may hold values from -0.75 to 0.75
- channel_decay_raw: float32 [2048], P('tp'), may hold values from 4.8 to 13.5
- token_decay_boost: float32 [4096, 2048], P('sp', 'tp'), may hold values from -0.7 to 0
- output_projection_weight: bfloat16 [2048, 2048], P('tp'), may hold values from -0.375 to 0.375
- expert_norm_gain: float32 [2048], replicated, may hold values from 0.1 to 1.9
- routes: int32 [4096, 2], P('sp'), may hold values from 0 to 7, all different within a row; in each aligned block of 128 rows (0 to 127, 128 to 255, ...) at most 48 rows name the same one
- expert_pair_weight: float32 [4096, 2], P(('sp', 'tp')), may hold values from 0.2 to 0.8
- gate_weight: bfloat16 [8, 2048, 2048], P('sp', None, 'tp'), may hold values from -0.125 to 0.125
- up_weight: bfloat16 [8, 2048, 2048], P('sp', None, 'tp'), may hold values from -0.125 to 0.125
- down_weight: bfloat16 [8, 2048, 2048], P('sp', None, 'tp'), may hold values from -0.25 to 0.25
Outputs:
- layer_out: bfloat16 [4096, 2048], P(('sp', 'tp'))
Inputs may be any that keep to these rules, and one draw needn't show every extreme that they name: `routes`: in each aligned block of 128 rows no expert is named by more than 48 rows, and the two experts of a row differ.
All inputs are finite; a program needn't handle non-finite values.
Results may differ from a plain program's by a relative error of at most 0.013.
Values may be sent and summed in bfloat16 or wider, within the bound.
A program may use at most 128 MiB of HBM per device.

v0:
```python
import functools

import jax
import jax.numpy as jnp
from jax import lax
from jax.experimental import pallas as pl
from jax.experimental.pallas import tpu as pltpu
from jax.sharding import PartitionSpec as P

RECURRENT_SCALE = 8.0
EPSILON = 1e-06
LANES = 128
TILE = 8
CHUNK = 64
RIM = 16
MESH = pl.DeviceIdType.MESH


def at_device(sp, tp):
    return {"device_id": (sp, tp), "device_id_type": MESH}


def one_minus_exp(y):
    series = 1.0 + y * (1 / 2 + y * (1 / 6 + y * (1 / 24 + y * (1 / 120 + y * (1 / 720 + y / 5040)))))
    series = series * -y
    return jnp.where(y > -0.4, series, 1.0 - jnp.exp(y))


def recurrence_kernel(
    sp_size,
    tp_size,
    x_hbm,
    out_gate_hbm,
    taps_hbm,
    recur_map_hbm,
    input_map_hbm,
    decay_hbm,
    boost_hbm,
    weight_hbm,
    resid_hbm,
    gain_hbm,
    stream_ref,
    normed_ref,
    x_ref,
    out_gate_ref,
    taps_ref,
    recur_map_ref,
    input_map_ref,
    decay_ref,
    boost_ref,
    weight_ref,
    resid_ref,
    gain_ref,
    gates_ref,
    ext,
    rim,
    running,
    local,
    lifted,
    totals,
    send_pair,
    recv_pair,
    send_far,
    recv_far,
    summed,
    load_sems,
    rim_sems,
    total_send_sems,
    total_recv_sems,
    pair_send_sems,
    pair_recv_sems,
    far_send_sems,
    far_recv_sems,
):
    sp, tp = lax.axis_index("sp"), lax.axis_index("tp")
    tokens, channels = x_ref.shape
    taps = taps_ref.shape[0]
    width = weight_ref.shape[1]
    rows_dev = resid_ref.shape[0]
    far_size = tp_size // 2
    core, far = lax.rem(tp, 2), tp // 2
    partner = far * 2 + 1 - core

    sources = (
        (x_hbm, x_ref),
        (out_gate_hbm, out_gate_ref),
        (taps_hbm, taps_ref),
        (recur_map_hbm, recur_map_ref),
        (input_map_hbm, input_map_ref),
        (decay_hbm, decay_ref),
        (boost_hbm, boost_ref),
        (weight_hbm, weight_ref),
        (resid_hbm, resid_ref),
        (gain_hbm, gain_ref),
    )
    loads = [
        pltpu.make_async_copy(source, target, load_sems.at[n])
        for n, (source, target) in enumerate(sources)
    ]
    for load in loads:
        load.start()

    barrier = pltpu.get_barrier_semaphore()
    for d in range(1, sp_size):
        pl.semaphore_signal(barrier, inc=1, **at_device(lax.rem(sp + d, sp_size), tp))
    pl.semaphore_signal(barrier, inc=1, **at_device(sp, partner))
    for d in range(1, far_size):
        pl.semaphore_signal(
            barrier, inc=1, **at_device(sp, lax.rem(far + d, far_size) * 2 + core)
        )
    pl.semaphore_wait(barrier, sp_size - 1 + far_size)

    loads[0].wait()
    rim_copy = pltpu.make_async_remote_copy(
        src_ref=x_ref.at[pl.ds(tokens - RIM, RIM)],
        dst_ref=rim,
        send_sem=rim_sems.at[0],
        recv_sem=rim_sems.at[1],
        **at_device(lax.rem(sp + 1, sp_size), tp),
    )
    rim_copy.start()
    loads[1].wait()

    @pl.loop(0, tokens // CHUNK)
    def _(i):
        r = pl.multiple_of(i * CHUNK, CHUNK)
        ext[pl.ds(r + TILE, CHUNK), :] = x_ref[pl.ds(r, CHUNK), :].astype(jnp.float32)
        lifted[pl.ds(r, CHUNK), :] = jax.nn.gelu(out_gate_ref[pl.ds(r, CHUNK), :].astype(jnp.float32))

    for load in loads[2:6]:
        load.wait()
    map_size = recur_map_ref.shape[1]
    per = LANES // map_size
    gates_ref[...] = jnp.zeros_like(gates_ref)
    for b in range(channels // LANES):
        for n in range(per):
            rows = slice(n * map_size, (n + 1) * map_size)
            for side, maps in enumerate((recur_map_ref, input_map_ref)):
                start = side * LANES + n * map_size
                gates_ref[b, rows, start : start + map_size] = maps[b * per + n]
    raw = decay_ref[...]
    small = jnp.exp(-jnp.abs(raw))
    series = small * (1 - small * (1 / 2 - small * (1 / 3 - small * (1 / 4 - small * (1 / 5 - small / 6)))))
    plus = jnp.maximum(-raw, 0.0) + jnp.where(small < 0.05, series, jnp.log(1.0 + small))
    scale = -RECURRENT_SCALE * plus

    rim_copy.wait()
    loads[6].wait()
    edge = rim[...].astype(jnp.float32)[RIM - TILE :, :]
    ext[0:TILE, :] = jnp.where(sp == 0, 0.0, edge)

    tile_row = lax.broadcasted_iota(jnp.int32, (CHUNK, LANES), 0) % TILE

    def chunk(i, carry):
        r = pl.multiple_of(i * CHUNK, CHUNK)
        out = []
        for b in range(channels // LANES):
            cols = slice(b * LANES, (b + 1) * LANES)
            win = ext[pl.ds(r, CHUNK + TILE), cols]
            base = TILE - taps + 1
            mixed = win[base : base + CHUNK] * taps_ref[0:1, cols]
            for k in range(1, taps):
                mixed = mixed + win[base + k : base + k + CHUNK] * taps_ref[k : k + 1, cols]
            smoothed = mixed.astype(jnp.bfloat16)
            both = jnp.dot(smoothed, gates_ref[b], preferred_element_type=jnp.float32)
            recur = jax.nn.sigmoid(both[:, :LANES])
            inward = jax.nn.sigmoid(both[:, LANES:])
            log_decay = recur * scale[0:1, cols] + boost_ref[pl.ds(r, CHUNK), cols]
            a = jnp.exp(log_decay)
            h = jnp.sqrt(one_minus_exp(2.0 * log_decay)) * (inward * smoothed.astype(jnp.float32))
            for s in (1, 2, 4):
                inside = tile_row >= s
                a_before = jnp.where(inside, pltpu.roll(a, s, 0), 1.0)
                h_before = jnp.where(inside, pltpu.roll(h, s, 0), 0.0)
                h = a * h_before + h
                a = a * a_before
            carry_a, carry_h = carry[2 * b], carry[2 * b + 1]
            for t in range(CHUNK // TILE):
                rows = slice(t * TILE, (t + 1) * TILE)
                h_t = h[rows] + a[rows] * carry_h
                a_t = a[rows] * carry_a
                running[pl.ds(r + t * TILE, TILE), cols] = a_t
                local[pl.ds(r + t * TILE, TILE), cols] = h_t
                carry_a, carry_h = a_t[TILE - 1 : TILE], h_t[TILE - 1 : TILE]
            out += [carry_a, carry_h]
        return tuple(out)

    ones, zeros = jnp.ones((1, LANES), jnp.float32), jnp.zeros((1, LANES), jnp.float32)
    last = lax.fori_loop(0, tokens // CHUNK, chunk, (ones, zeros) * (channels // LANES))
    pick = lax.broadcasted_iota(jnp.int32, (TILE, LANES), 0) == 0
    for b in range(channels // LANES):
        totals[sp, :, b * LANES : (b + 1) * LANES] = jnp.where(pick, last[2 * b], last[2 * b + 1])

    sent = []
    for d in range(1, sp_size):
        copy = pltpu.make_async_remote_copy(
            src_ref=totals.at[sp],
            dst_ref=totals.at[sp],
            send_sem=total_send_sems.at[d],
            recv_sem=total_recv_sems.at[d],
            **at_device(lax.rem(sp + d, sp_size), tp),
        )
        copy.start()
        sent.append(copy)
    for copy in sent:
        copy.wait()

    entering = jnp.zeros((1, channels), jnp.float32)
    for k in range(sp_size):
        part = totals[k]
        after = part[0:1] * entering + part[1:2]
        entering = jnp.where(k < sp, after, entering)

    def partial_sum(block, n, step):
        rows = pl.ds(pl.multiple_of(block * rows_dev, rows_dev), rows_dev)
        state = local[rows, :] + running[rows, :] * entering
        branch = (lifted[rows, :] * state).astype(jnp.bfloat16)
        cols = slice(n * step, (n + 1) * step)
        return jnp.dot(branch, weight_ref[:, cols], preferred_element_type=jnp.float32)

    step = 512 if width % 512 == 0 else width
    steps = width // step

    for load in loads[7:]:
        load.wait()
    pair_copies = {}
    for d in range(1, far_size + 1):
        other = lax.rem(far + d, far_size)
        for n in range(steps):
            send_pair[d - 1, n] = partial_sum(other * 2 + 1 - core, n, step).astype(jnp.bfloat16)
            pair_copies[d, n] = pltpu.make_async_remote_copy(
                src_ref=send_pair.at[d - 1, n],
                dst_ref=recv_pair.at[d - 1, n],
                send_sem=pair_send_sems.at[d - 1, n],
                recv_sem=pair_recv_sems.at[d - 1, n],
                **at_device(sp, partner),
            )
            pair_copies[d, n].start()
    far_copies = {}
    for d in range(1, far_size):
        other = lax.rem(far + d, far_size)
        for n in range(steps):
            total = partial_sum(other * 2 + core, n, step)
            pair_copies[d, n].wait_recv()
            total = total + recv_pair[d - 1, n].astype(jnp.float32)
            send_far[d - 1, n] = total.astype(jnp.bfloat16)
            far_copies[d, n] = pltpu.make_async_remote_copy(
                src_ref=send_far.at[d - 1, n],
                dst_ref=recv_far.at[d - 1, n],
                send_sem=far_send_sems.at[d - 1, n],
                recv_sem=far_recv_sems.at[d - 1, n],
                **at_device(sp, other * 2 + core),
            )
            far_copies[d, n].start()

    for n in range(steps):
        cols = slice(n * step, (n + 1) * step)
        total = partial_sum(tp, n, step) + resid_ref[:, cols].astype(jnp.float32)
        pair_copies[far_size, n].wait_recv()
        summed[:, cols] = total + recv_pair[far_size - 1, n].astype(jnp.float32)

    squares = jnp.zeros((rows_dev, 1), jnp.float32)
    for n in range(steps):
        cols = slice(n * step, (n + 1) * step)
        total = summed[:, cols]
        for d in range(1, far_size):
            far_copies[d, n].wait_recv()
            total = total + recv_far[d - 1, n].astype(jnp.float32)
        stream = total.astype(jnp.bfloat16)
        stream_ref[:, cols] = stream
        wide = stream.astype(jnp.float32)
        squares = squares + jnp.sum(wide * wide, axis=1, keepdims=True)
    norm = lax.rsqrt(squares * (1.0 / width) + EPSILON)
    for n in range(steps):
        cols = slice(n * step, (n + 1) * step)
        wide = stream_ref[:, cols].astype(jnp.float32)
        normed_ref[:, cols] = (wide * norm * gain_ref[0:1, cols]).astype(jnp.bfloat16)
    for copy in [*pair_copies.values(), *far_copies.values()]:
        copy.wait_send()


def recurrence(
    resid,
    recurrent_input,
    recurrent_out_gate,
    filter_weight,
    recurrence_gate_matrix,
    input_gate_matrix,
    channel_decay_raw,
    token_decay_boost,
    output_projection_weight,
    expert_norm_gain,
):
    sp_size, tp_size = lax.axis_size("sp"), lax.axis_size("tp")
    tokens, channels = recurrent_input.shape
    rows_dev, width = resid.shape
    far_size = tp_size // 2
    step = 512 if width % 512 == 0 else width
    steps = width // step
    vmem = pl.BlockSpec(memory_space=pltpu.VMEM)
    row_shape = jax.ShapeDtypeStruct((rows_dev, width), jnp.bfloat16)
    wide = pltpu.VMEM((tokens, channels), jnp.float32)
    far_slots = max(1, far_size - 1)
    operands = (
        recurrent_input,
        recurrent_out_gate,
        filter_weight,
        recurrence_gate_matrix,
        input_gate_matrix,
        channel_decay_raw.reshape(1, channels),
        token_decay_boost,
        output_projection_weight,
        resid,
        expert_norm_gain.reshape(1, width),
    )
    return pl.pallas_call(
        functools.partial(recurrence_kernel, sp_size, tp_size),
        out_shape=(row_shape, row_shape),
        in_specs=[pl.BlockSpec(memory_space=pltpu.HBM)] * len(operands),
        out_specs=(vmem, vmem),
        scratch_shapes=[
            *[pltpu.VMEM(operand.shape, operand.dtype) for operand in operands],
            pltpu.VMEM((channels // LANES, LANES, 2 * LANES), jnp.bfloat16),
            pltpu.VMEM((tokens + TILE, channels), jnp.float32),
            pltpu.VMEM((RIM, channels), jnp.bfloat16),
            wide,
            wide,
            wide,
            pltpu.VMEM((sp_size, TILE, channels), jnp.float32),
            pltpu.VMEM((far_size, steps, rows_dev, step), jnp.bfloat16),
            pltpu.VMEM((far_size, steps, rows_dev, step), jnp.bfloat16),
            pltpu.VMEM((far_slots, steps, rows_dev, step), jnp.bfloat16),
            pltpu.VMEM((far_slots, steps, rows_dev, step), jnp.bfloat16),
            pltpu.VMEM((rows_dev, width), jnp.float32),
            pltpu.SemaphoreType.DMA((len(operands),)),
            pltpu.SemaphoreType.DMA((2,)),
            pltpu.SemaphoreType.DMA((sp_size,)),
            pltpu.SemaphoreType.DMA((sp_size,)),
            pltpu.SemaphoreType.DMA((far_size, steps)),
            pltpu.SemaphoreType.DMA((far_size, steps)),
            pltpu.SemaphoreType.DMA((far_slots, steps)),
            pltpu.SemaphoreType.DMA((far_slots, steps)),
        ],
        compiler_params=pltpu.CompilerParams(
            collective_id=0, has_side_effects=True, vmem_limit_bytes=67043328
        ),
    )(*operands)


def slot_numbers(picks, experts):
    flat = picks.reshape(-1)
    onehot = (flat[:, None] == jnp.arange(experts, dtype=jnp.int32)[None, :]).astype(jnp.int32)
    before = jnp.cumsum(onehot, axis=0) - onehot
    return (flat, jnp.sum(before * onehot, axis=1))


def fill_slots(source_rows, slot_of, row_of, slot_count):
    match = slot_of[None, :] == jnp.arange(slot_count, dtype=jnp.int32)[:, None]
    picked = jnp.sum(jnp.where(match, row_of[None, :], 0), axis=1)
    present = jnp.any(match, axis=1)
    return jnp.where(present[:, None], source_rows[picked], jnp.zeros((), source_rows.dtype))


def expert_hidden(rows, gate_weight, up_weight):
    gate = jnp.dot(rows, gate_weight[0], preferred_element_type=jnp.float32)
    upward = jnp.dot(rows, up_weight[0], preferred_element_type=jnp.float32)
    return (jax.nn.silu(gate) * upward).astype(jnp.bfloat16)


def expert_down(active, down_weight):
    columns = down_weight[0]
    return jnp.dot(
        lax.all_gather(active, "tp", axis=1, tiled=True),
        columns,
        preferred_element_type=jnp.float32,
    ).astype(jnp.bfloat16)


def experts_kernel(
    sp_size,
    tp_size,
    capacity,
    normed_ref,
    stream_ref,
    routes_ref,
    pair_weight_ref,
    gate_hbm,
    up_hbm,
    down_hbm,
    out_ref,
    gate,
    up,
    down,
    outgoing,
    rows,
    active,
    result,
    returned,
    blend,
    gathered,
    pair_weights,
    ranks,
    mixers,
    load_sems,
    weight_send,
    weight_recv,
    out_send,
    out_recv,
    row_pair_send,
    row_pair_recv,
    row_far_send,
    row_far_recv,
    act_pair_send,
    act_pair_recv,
    act_far_send,
    act_far_recv,
    back_send,
    back_recv,
    blend_send,
    blend_recv,
):
    sp, tp = lax.axis_index("sp"), lax.axis_index("tp")
    rows_dev, width = normed_ref.shape
    picks = routes_ref.shape[1]
    hidden, columns = gate.shape[1], down.shape[1]
    far_size = tp_size // 2
    core, far = lax.rem(tp, 2), tp // 2
    partner = far * 2 + 1 - core

    loads = [
        pltpu.make_async_copy(source.at[0], target, load_sems.at[n])
        for n, (source, target) in enumerate(((gate_hbm, gate), (up_hbm, up), (down_hbm, down)))
    ]
    for load in loads:
        load.start()

    barrier = pltpu.get_barrier_semaphore()
    for d in range(1, sp_size):
        pl.semaphore_signal(barrier, inc=1, **at_device(lax.rem(sp + d, sp_size), tp))
    for u in range(1, tp_size):
        pl.semaphore_signal(barrier, inc=1, **at_device(sp, lax.rem(tp + u, tp_size)))

    slot_row = lax.broadcasted_iota(jnp.int32, (capacity, rows_dev), 0)

    expert_row = lax.broadcasted_iota(jnp.int32, (sp_size, rows_dev), 0)
    earlier = lax.broadcasted_iota(jnp.int32, (rows_dev, rows_dev), 0) < lax.broadcasted_iota(
        jnp.int32, (rows_dev, rows_dev), 1
    )
    earlier = jnp.where(earlier, 1.0, 0.0).astype(jnp.bfloat16)

    def rank_block(block):
        chosen = routes_ref[block]
        hits = jnp.zeros((sp_size, rows_dev), jnp.float32)
        for k in range(picks):
            hits = hits + jnp.where(expert_row == chosen[k : k + 1], 1.0, 0.0)
        ranks[block] = jnp.dot(
            hits.astype(jnp.bfloat16), earlier, preferred_element_type=jnp.float32
        )

    def selector(block, expert, values):
        chosen = routes_ref[block]
        value = jnp.zeros((1, rows_dev), jnp.float32)
        for k in range(picks):
            value = value + jnp.where(chosen[k : k + 1] == expert, values[k : k + 1], 0.0)
        rank = ranks[block, pl.ds(expert, 1), :].astype(jnp.int32)
        return jnp.where(rank == slot_row, value, 0.0)

    def packed(expert):
        ones = jnp.ones((picks, rows_dev), jnp.float32)
        choose = selector(tp, expert, ones).astype(jnp.bfloat16)
        return jnp.dot(choose, normed_ref[...], preferred_element_type=jnp.float32).astype(
            jnp.bfloat16
        )

    def slot_rows(block):
        return pl.ds(pl.multiple_of(block * capacity, capacity), capacity)

    def source_of(d):
        return lax.rem(sp - d + sp_size, sp_size)

    def far_tp(j):
        return lax.rem(far - j + far_size, far_size) * 2 + core

    def weight_copy(u):
        return pltpu.make_async_remote_copy(
            src_ref=pair_weight_ref,
            dst_ref=pair_weights.at[tp],
            send_sem=weight_send.at[u],
            recv_sem=weight_recv.at[u],
            **at_device(sp, lax.rem(tp + u, tp_size)),
        )

    def out_copy(d):
        return pltpu.make_async_remote_copy(
            src_ref=outgoing.at[d],
            dst_ref=rows.at[sp, slot_rows(tp)],
            send_sem=out_send.at[d],
            recv_sem=out_recv.at[d],
            **at_device(lax.rem(sp + d, sp_size), tp),
        )

    def row_pair(d, j):
        place = rows.at[source_of(d), slot_rows(far_tp(j))]
        return pltpu.make_async_remote_copy(
            src_ref=place,
            dst_ref=place,
            send_sem=row_pair_send.at[d, j],
            recv_sem=row_pair_recv.at[d, j],
            **at_device(sp, partner),
        )

    def row_far(d, j):
        place = rows.at[source_of(d), slot_rows(tp)]
        return pltpu.make_async_remote_copy(
            src_ref=place,
            dst_ref=place,
            send_sem=row_far_send.at[d, j],
            recv_sem=row_far_recv.at[d, j],
            **at_device(sp, lax.rem(far + j, far_size) * 2 + core),
        )

    def act_pair(d, j):
        place = active.at[source_of(d), far_tp(j)]
        return pltpu.make_async_remote_copy(
            src_ref=place,
            dst_ref=place,
            send_sem=act_pair_send.at[d, j],
            recv_sem=act_pair_recv.at[d, j],
            **at_device(sp, partner),
        )

    def act_far(d, j):
        place = active.at[source_of(d), tp]
        return pltpu.make_async_remote_copy(
            src_ref=place,
            dst_ref=place,
            send_sem=act_far_send.at[d, j],
            recv_sem=act_far_recv.at[d, j],
            **at_device(sp, lax.rem(far + j, far_size) * 2 + core),
        )

    def back_copy(d):
        return pltpu.make_async_remote_copy(
            src_ref=result.at[d],
            dst_ref=returned.at[sp],
            send_sem=back_send.at[d],
            recv_sem=back_recv.at[d],
            **at_device(source_of(d), tp),
        )

    def blend_copy(u):
        return pltpu.make_async_remote_copy(
            src_ref=blend.at[u],
            dst_ref=gathered.at[tp],
            send_sem=blend_send.at[u],
            recv_sem=blend_recv.at[u],
            **at_device(sp, lax.rem(tp + u, tp_size)),
        )

    rank_block(tp)
    rows[sp, slot_rows(tp), :] = packed(sp)
    pair_weights[tp] = pair_weight_ref[...]
    pl.semaphore_wait(barrier, sp_size - 1 + tp_size - 1)
    for j in range(1, far_size):
        row_far(0, j).start()
    row_pair(0, 0).start()

    @pl.loop(1, sp_size)
    def _(d):
        outgoing[d] = packed(lax.rem(sp + d, sp_size))
        out_copy(d).start()

    for u in range(1, tp_size):
        weight_copy(u).start()

    for load in loads:
        load.wait()

    @pl.loop(0, sp_size + 4)
    def _(step):
        @pl.when((step > 0) & (step < sp_size))
        def _():
            out_copy(step).wait_recv()
            for j in range(1, far_size):
                row_far(step, j).start()
            row_pair(step, 0).start()

        @pl.when((step >= 2) & (step < sp_size + 2))
        def _():
            d = step - 2
            for j in range(far_size):
                row_pair(d, j).wait_recv()
            source = source_of(d)
            given = rows[source]
            gated = jnp.dot(given, gate[...], preferred_element_type=jnp.float32)
            upward = jnp.dot(given, up[...], preferred_element_type=jnp.float32)
            active[source, tp] = (jax.nn.silu(gated) * upward).astype(jnp.bfloat16)
            for j in range(1, far_size):
                act_far(d, j).start()
            act_pair(d, 0).start()

        @pl.when((step >= 3) & (step < sp_size + 3))
        def _():
            for j in range(1, far_size):
                act_far(step - 3, j).wait_recv()
                act_pair(step - 3, j).start()

        @pl.when((step >= 1) & (step < sp_size + 1))
        def _():
            for j in range(1, far_size):
                row_far(step - 1, j).wait_recv()
                row_pair(step - 1, j).start()

        for u in range(1, tp_size):

            @pl.when(step == 3)
            def _(u=u):
                weight_copy(u).wait_recv()
                rank_block(lax.rem(tp + u, tp_size))

        @pl.when(step >= 4)
        def _():
            d = step - 4
            for j in range(far_size):
                act_pair(d, j).wait_recv()
            source = source_of(d)
            total = jnp.dot(
                active[source, 0], down[0:hidden, :], preferred_element_type=jnp.float32
            )
            for t in range(1, tp_size):
                total = total + jnp.dot(
                    active[source, t],
                    down[t * hidden : (t + 1) * hidden, :],
                    preferred_element_type=jnp.float32,
                )
            result[d] = total.astype(jnp.bfloat16)

            @pl.when(d == 0)
            def _():
                returned[sp] = total.astype(jnp.bfloat16)

            @pl.when(d > 0)
            def _():
                back_copy(d).start()

            @pl.when(d < tp_size)
            def _():
                weight = pair_weights[d]
                coarse = weight.astype(jnp.bfloat16).astype(jnp.float32)
                for n, values in enumerate((coarse, weight - coarse)):
                    picked = [selector(d, e, values) for e in range(sp_size)]
                    mixers[d, n] = jnp.concatenate(picked, axis=0).T.astype(jnp.bfloat16)

    @pl.loop(1, sp_size)
    def _(d):
        back_copy(d).wait_recv()

    def blended(block):
        part = returned[:, slot_rows(block), :].reshape(sp_size * capacity, columns)
        total = jnp.dot(mixers[block, 0], part, preferred_element_type=jnp.float32)
        total = total + jnp.dot(mixers[block, 1], part, preferred_element_type=jnp.float32)
        return total.astype(jnp.bfloat16)

    for u in [*range(2, tp_size), 1]:
        blend[u] = blended(lax.rem(tp + u, tp_size))
        blend_copy(u).start()

    gathered[tp] = blended(tp)
    for u in range(1, tp_size):
        blend_copy(u).wait_recv()
    for t in range(tp_size):
        cols = slice(t * columns, (t + 1) * columns)
        out_ref[:, cols] = (
            stream_ref[:, cols].astype(jnp.float32) + gathered[t].astype(jnp.float32)
        ).astype(jnp.bfloat16)

    for u in range(1, tp_size):
        weight_copy(u).wait_send()
        blend_copy(u).wait_send()

    @pl.loop(1, sp_size)
    def _(d):
        out_copy(d).wait_send()
        back_copy(d).wait_send()

    @pl.loop(0, sp_size)
    def _(d):
        for j in range(far_size):
            row_pair(d, j).wait_send()
            act_pair(d, j).wait_send()
        for j in range(1, far_size):
            row_far(d, j).wait_send()
            act_far(d, j).wait_send()


def routed_experts(
    normed, stream, routes, expert_pair_weight, gate_weight, up_weight, down_weight, capacity
):
    sp_size, tp_size = lax.axis_size("sp"), lax.axis_size("tp")
    rows_dev, width = normed.shape
    hidden, columns = gate_weight.shape[2], down_weight.shape[2]
    by_block = routes.reshape(tp_size, rows_dev, -1).swapaxes(1, 2)
    pair_weight = jnp.pad(expert_pair_weight.T, ((0, TILE - expert_pair_weight.shape[1]), (0, 0)))
    vmem = pl.BlockSpec(memory_space=pltpu.VMEM)
    anywhere = pl.BlockSpec(memory_space=pl.ANY)
    far_size = tp_size // 2

    def buffer(*shape):
        return pltpu.VMEM(shape, jnp.bfloat16)

    slots_all = tp_size * capacity
    dma = pltpu.SemaphoreType.DMA
    return pl.pallas_call(
        functools.partial(experts_kernel, sp_size, tp_size, capacity),
        out_shape=jax.ShapeDtypeStruct((rows_dev, width), jnp.bfloat16),
        in_specs=[vmem] * 4 + [anywhere] * 3,
        out_specs=vmem,
        scratch_shapes=[
            buffer(*gate_weight.shape[1:]),
            buffer(*up_weight.shape[1:]),
            buffer(*down_weight.shape[1:]),
            buffer(sp_size, capacity, width),
            buffer(sp_size, slots_all, width),
            buffer(sp_size, tp_size, slots_all, hidden),
            buffer(sp_size, slots_all, columns),
            buffer(sp_size, slots_all, columns),
            buffer(tp_size, rows_dev, columns),
            buffer(tp_size, rows_dev, columns),
            pltpu.VMEM((tp_size, TILE, rows_dev), jnp.float32),
            pltpu.VMEM((tp_size, sp_size, rows_dev), jnp.float32),
            buffer(tp_size, 2, rows_dev, sp_size * capacity),
            dma((3,)),
            dma((tp_size,)),
            dma((tp_size,)),
            dma((sp_size,)),
            dma((sp_size,)),
            *[dma((sp_size, far_size))] * 8,
            dma((sp_size,)),
            dma((sp_size,)),
            dma((tp_size,)),
            dma((tp_size,)),
        ],
        compiler_params=pltpu.CompilerParams(
            collective_id=1, has_side_effects=True, vmem_limit_bytes=67043328
        ),
    )(normed, stream, by_block, pair_weight, gate_weight, up_weight, down_weight)


def body(
    resid,
    recurrent_input,
    recurrent_out_gate,
    filter_weight,
    recurrence_gate_matrix,
    input_gate_matrix,
    channel_decay_raw,
    token_decay_boost,
    output_projection_weight,
    expert_norm_gain,
    routes,
    expert_pair_weight,
    gate_weight,
    up_weight,
    down_weight,
):
    tp_size = lax.axis_size("tp")
    stream, normed = recurrence(
        resid,
        recurrent_input,
        recurrent_out_gate,
        filter_weight,
        recurrence_gate_matrix,
        input_gate_matrix,
        channel_decay_raw,
        token_decay_boost,
        output_projection_weight,
        expert_norm_gain,
    )
    stream_wide = stream.astype(jnp.float32)
    rows_dev = stream.shape[0]
    model_width = normed.shape[1]
    experts = lax.axis_size("sp")
    capacity = max(2, 3 * rows_dev // experts)
    if capacity % RIM == 0 and rows_dev % LANES == 0 and tp_size <= experts:
        return routed_experts(
            normed,
            stream,
            routes,
            expert_pair_weight,
            gate_weight,
            up_weight,
            down_weight,
            capacity,
        )
    own_routes = lax.dynamic_slice_in_dim(routes, lax.axis_index("tp") * rows_dev, rows_dev, 0)
    own_flat, own_rank = slot_numbers(own_routes, experts)
    own_slots = own_flat * capacity + own_rank
    row_of = jnp.arange(2 * rows_dev, dtype=jnp.int32) // 2
    outgoing = fill_slots(normed, own_slots, row_of, experts * capacity).reshape(
        experts, capacity, model_width
    )
    arrived = lax.all_to_all(outgoing, "sp", split_axis=0, concat_axis=0, tiled=True)
    piece = lax.all_gather(
        arrived.reshape(1, experts * capacity, model_width), "tp", axis=0, tiled=True
    )
    flat_rows = piece.reshape(piece.shape[0] * piece.shape[1], model_width)
    active = expert_hidden(flat_rows, gate_weight, up_weight).reshape(
        piece.shape[0], piece.shape[1], -1
    )
    result = expert_down(active.reshape(-1, active.shape[2]), down_weight)
    joined = lax.all_to_all(
        result.reshape(tp_size, experts * capacity, -1),
        "tp",
        split_axis=0,
        concat_axis=2,
        tiled=True,
    )
    returned = lax.all_to_all(
        joined.reshape(experts, capacity, model_width),
        "sp",
        split_axis=0,
        concat_axis=0,
        tiled=True,
    )
    picked = (
        returned.reshape(experts * capacity, model_width)[own_slots]
        .astype(jnp.float32)
        .reshape(rows_dev, 2, model_width)
    )
    blended = jnp.sum(picked * expert_pair_weight[:, :, None], axis=1)
    return (stream_wide + blended).astype(jnp.bfloat16)


def solution(mesh):
    placed = (
        P(("sp", "tp"), None),
        P("sp", "tp"),
        P("sp", "tp"),
        P(None, "tp"),
        P("tp", None, None),
        P("tp", None, None),
        P("tp"),
        P("sp", "tp"),
        P("tp", None),
        P(),
        P("sp", None),
        P(("sp", "tp"), None),
        P("sp", None, "tp"),
        P("sp", None, "tp"),
        P("sp", None, "tp"),
    )
    return jax.shard_map(
        body, mesh=mesh, in_specs=placed, out_specs=P(("sp", "tp"), None), check_vma=False
    )
```

profile of v0, /device:TPU:0, one launch (start us, length us, event | category | flops | bytes accessed | tf_op | source)
XLA Modules:
  0.0 148.7 jit_solution(9278532675789662461)
XLA Ops:
  0.0 1.3 pad.4.pair_weight_ref
  1.3 33.5 %shard_map.145 = (bf16[128,2048]{1,0:T(8,128)(2,1)}, bf16[128,2048]{1,0:T(8,128)(2,1)}) custom-call(bf16[512,512]{1,0:T(8,128)(2,1)} %x_hbm.1, bf16[512,512]{1,0:T(8,128)(2,1)} %out_gate_hbm.1, f32[4,512]{1,0:T(4,128)} %taps_hbm.1, bf16[8,64,64]{2,1,0:T(8,128)(2,1)} %recur_map_hbm.1, bf16[8,64,64]{2,1,0:T(8,128)(2,1)} %input_map_hbm.1, f32[1,512]{1,0:T(1,128)} %bitcast.8, ...), custom_call_target="tpu_custom_call" | custom-call | tf_op jit(solution)/shard_map/pallas_call | solution.py:316
  34.8 112.0 %shard_map.146 = bf16[128,2048]{1,0:T(8,128)(2,1)} custom-call(bf16[128,2048]{1,0:T(8,128)(2,1)} %get-tuple-element.7.normed_ref, bf16[128,2048]{1,0:T(8,128)(2,1)} %get-tuple-element.8.stream_ref, s32[4,2,128]{2,1,0:T(2,128)} %bitcast.7, f32[8,128]{1,0:T(8,128)} %pad.4.pair_weight_ref, bf16[1,2048,512]{2,1,0:T(8,128)(2,1)} %gate_hbm.1, ...), custom_call_target="tpu_custom_call" | custom-call | tf_op jit(solution)/shard_map/pallas_call | solution.py:713
  146.8 1.9 %copy.17 = bf16[128,2048]{1,0:T(8,128)(2,1)} copy(bf16[128,2048]{1,0:T(8,128)(2,1)} %shard_map.146) | data formatting | bytes 1048576
where the time goes:
time: 150 us; the launch traced here: 149 us
  Pallas kernels  145 us (97%)
  local copies, waits for them, and re-layouts  3.16 us (2%)
    pallas_call x1, Pallas kernels, routed_experts(): pl.pallas_call(functools.partial(experts_kernel, sp_size, tp_size, capaci...  112 us
    pallas_call x1, Pallas kernels, recurrence(): pl.pallas_call(functools.partial(recurrence_kernel, sp_size, tp_size), ou...  33.5 us

commit v1 on v0

--- a/solution.py
+++ b/solution.py
@@ -1,3 +1,4 @@
+import contextlib
 import functools
 
 import jax
@@ -376,62 +377,150 @@
     ).astype(jnp.bfloat16)
 
 
-def experts_kernel(
+def phase(name):
+    return contextlib.nullcontext()
+
+
+def layer_kernel(
     sp_size,
     tp_size,
     capacity,
-    normed_ref,
-    stream_ref,
-    routes_ref,
-    pair_weight_ref,
+    x_hbm,
+    out_gate_hbm,
+    taps_hbm,
+    recur_map_hbm,
+    input_map_hbm,
+    decay_hbm,
+    boost_hbm,
+    routes_hbm,
+    pair_weight_hbm,
+    weight_hbm,
+    resid_hbm,
+    gain_hbm,
     gate_hbm,
     up_hbm,
     down_hbm,
     out_ref,
+    x_ref,
+    out_gate_ref,
+    taps_ref,
+    recur_map_ref,
+    input_map_ref,
+    decay_ref,
+    boost_ref,
+    routes_ref,
+    pair_weight_ref,
+    weight_ref,
+    resid_ref,
+    gain_ref,
     gate,
     up,
     down,
+    gates_ref,
+    ext,
+    rim,
+    running,
+    local,
+    lifted,
+    branch,
+    totals,
+    across,
+    along,
+    send_pair,
+    recv_pair,
+    send_far,
+    recv_far,
+    summed,
+    stream_ref,
+    normed_ref,
+    other_normed,
+    own_weights,
+    pair_weights,
+    ranks,
+    choose,
+    choose_other,
+    mixers,
     outgoing,
+    outgoing_other,
     rows,
     active,
     result,
     returned,
     blend,
     gathered,
-    pair_weights,
-    ranks,
-    mixers,
     load_sems,
+    rim_sems,
+    total_send,
+    total_recv,
+    pair_send,
+    pair_recv,
+    far_send,
+    far_recv,
+    cross_send,
+    cross_recv,
     weight_send,
     weight_recv,
     out_send,
     out_recv,
+    near_send,
+    near_recv,
+    row_far_send,
+    row_far_recv,
     row_pair_send,
     row_pair_recv,
-    row_far_send,
-    row_far_recv,
+    act_far_send,
+    act_far_recv,
     act_pair_send,
     act_pair_recv,
-    act_far_send,
-    act_far_recv,
     back_send,
     back_recv,
     blend_send,
     blend_recv,
 ):
     sp, tp = lax.axis_index("sp"), lax.axis_index("tp")
-    rows_dev, width = normed_ref.shape
+    tokens, channels = x_ref.shape
+    taps = taps_ref.shape[0]
+    rows_dev, width = resid_ref.shape
     picks = routes_ref.shape[1]
     hidden, columns = gate.shape[1], down.shape[1]
-    far_size = tp_size // 2
     core, far = lax.rem(tp, 2), tp // 2
+    other = 1 - far
     partner = far * 2 + 1 - core
-
+    across_tp = other * 2 + core
+    half = sp_size // 2
+    steps, step = send_pair.shape[1], send_pair.shape[3]
+    pieces = far_send.shape[0]
+    piece = rows_dev // pieces
+
+    def flipped(d):
+        total, bit = 0, 1
+        while bit < sp_size:
+            total = total + bit * lax.rem(sp // bit + d // bit, 2)
+            bit *= 2
+        return total
+
+    sources = (
+        (x_hbm, x_ref),
+        (out_gate_hbm, out_gate_ref),
+        (taps_hbm, taps_ref),
+        (recur_map_hbm, recur_map_ref),
+        (input_map_hbm, input_map_ref),
+        (decay_hbm, decay_ref),
+        (boost_hbm, boost_ref),
+        (routes_hbm, routes_ref),
+        (pair_weight_hbm, pair_weight_ref),
+        (weight_hbm, weight_ref),
+        (resid_hbm, resid_ref),
+        (gain_hbm, gain_ref),
+        (gate_hbm.at[0], gate),
+        (up_hbm.at[0], up),
+        (down_hbm.at[0], down),
+    )
     loads = [
-        pltpu.make_async_copy(source.at[0], target, load_sems.at[n])
-        for n, (source, target) in enumerate(((gate_hbm, gate), (up_hbm, up), (down_hbm, down)))
+        pltpu.make_async_copy(source, target, load_sems.at[n])
+        for n, (source, target) in enumerate(sources)
     ]
-    for load in loads:
+    for load in loads[:12]:
         load.start()
 
     barrier = pltpu.get_barrier_semaphore()
@@ -440,22 +529,239 @@
     for u in range(1, tp_size):
         pl.semaphore_signal(barrier, inc=1, **at_device(sp, lax.rem(tp + u, tp_size)))
 
+    loads[0].wait()
+    chunks = tokens // CHUNK
+
+    @pl.loop(0, chunks)
+    def _(i):
+        r = pl.multiple_of(i * CHUNK, CHUNK)
+        ext[pl.ds(r + TILE, CHUNK), :] = x_ref[pl.ds(r, CHUNK), :].astype(jnp.float32)
+
+    for load in loads[2:6]:
+        load.wait()
+    map_size = recur_map_ref.shape[1]
+    per = LANES // map_size
+    gates_ref[...] = jnp.zeros_like(gates_ref)
+    for b in range(channels // LANES):
+        for n in range(per):
+            spots = slice(n * map_size, (n + 1) * map_size)
+            for side, maps in enumerate((recur_map_ref, input_map_ref)):
+                start = side * LANES + n * map_size
+                gates_ref[b, spots, start : start + map_size] = maps[b * per + n]
+    raw = decay_ref[...]
+    small = jnp.exp(-jnp.abs(raw))
+    series = small * (1 - small * (1 / 2 - small * (1 / 3 - small * (1 / 4 - small * (1 / 5 - small / 6)))))
+    plus = jnp.maximum(-raw, 0.0) + jnp.where(small < 0.05, series, jnp.log(1.0 + small))
+    scale = -RECURRENT_SCALE * plus
+
+    loads[8].wait()
+    own_weights[...] = jnp.zeros_like(own_weights)
+    own_weights[0:picks, :] = pair_weight_ref[...]
+    pair_weights[tp] = own_weights[...]
+
+    with phase("barrier"):
+        pl.semaphore_wait(barrier, sp_size - 1 + tp_size - 1)
+    rim_copy = pltpu.make_async_remote_copy(
+        src_ref=x_ref.at[pl.ds(tokens - RIM, RIM)],
+        dst_ref=rim,
+        send_sem=rim_sems.at[0],
+        recv_sem=rim_sems.at[1],
+        **at_device(lax.rem(sp + 1, sp_size), tp),
+    )
+    rim_copy.start()
+
+    def weight_copy(u):
+        return pltpu.make_async_remote_copy(
+            src_ref=own_weights,
+            dst_ref=pair_weights.at[tp],
+            send_sem=weight_send.at[u],
+            recv_sem=weight_recv.at[u],
+            **at_device(sp, lax.rem(tp + u, tp_size)),
+        )
+
+    for u in range(1, tp_size):
+        weight_copy(u).start()
+    loads[6].wait()
+    for load in loads[12:]:
+        load.start()
+
+    tile_row = lax.broadcasted_iota(jnp.int32, (CHUNK, LANES), 0) % TILE
+
+    def chunk(i, carry):
+        r = pl.multiple_of(i * CHUNK, CHUNK)
+        out = []
+        for b in range(channels // LANES):
+            cols = slice(b * LANES, (b + 1) * LANES)
+            win = ext[pl.ds(r, CHUNK + TILE), cols]
+            base = TILE - taps + 1
+            mixed = win[base : base + CHUNK] * taps_ref[0:1, cols]
+            for k in range(1, taps):
+                mixed = mixed + win[base + k : base + k + CHUNK] * taps_ref[k : k + 1, cols]
+            smoothed = mixed.astype(jnp.bfloat16)
+            both = jnp.dot(smoothed, gates_ref[b], preferred_element_type=jnp.float32)
+            recur = jax.nn.sigmoid(both[:, :LANES])
+            inward = jax.nn.sigmoid(both[:, LANES:])
+            log_decay = recur * scale[0:1, cols] + boost_ref[pl.ds(r, CHUNK), cols]
+            a = jnp.exp(log_decay)
+            h = jnp.sqrt(one_minus_exp(2.0 * log_decay)) * (inward * smoothed.astype(jnp.float32))
+            for s in (1, 2, 4):
+                inside = tile_row >= s
+                a_before = jnp.where(inside, pltpu.roll(a, s, 0), 1.0)
+                h_before = jnp.where(inside, pltpu.roll(h, s, 0), 0.0)
+                h = a * h_before + h
+                a = a * a_before
+            carry_a, carry_h = carry[2 * b], carry[2 * b + 1]
+            for t in range(CHUNK // TILE):
+                spots = slice(t * TILE, (t + 1) * TILE)
+                h_t = h[spots] + a[spots] * carry_h
+                a_t = a[spots] * carry_a
+                running[pl.ds(r + t * TILE, TILE), cols] = a_t
+                local[pl.ds(r + t * TILE, TILE), cols] = h_t
+                carry_a, carry_h = a_t[TILE - 1 : TILE], h_t[TILE - 1 : TILE]
+            out += [carry_a, carry_h]
+        return tuple(out)
+
+    ones, zeros = jnp.ones((1, LANES), jnp.float32), jnp.zeros((1, LANES), jnp.float32)
+    start = (ones, zeros) * (channels // LANES)
+    with phase("scan"):
+        rest = lax.fori_loop(1, chunks, chunk, start)
+    with phase("rim"):
+        rim_copy.wait()
+    edge = rim[...].astype(jnp.float32)[RIM - TILE :, :]
+    ext[0:TILE, :] = jnp.where(sp == 0, 0.0, edge)
+    with phase("head"):
+        first = lax.fori_loop(0, 1, chunk, start)
+    pick = lax.broadcasted_iota(jnp.int32, (TILE, LANES), 0) == 0
+    for b in range(channels // LANES):
+        first_a, first_h, rest_a, rest_h = first[2 * b], first[2 * b + 1], rest[2 * b], rest[2 * b + 1]
+        totals[sp, :, b * LANES : (b + 1) * LANES] = jnp.where(
+            pick, first_a * rest_a, rest_a * first_h + rest_h
+        )
+    head_a = jnp.concatenate(first[0::2], axis=1)
+    head_h = jnp.concatenate(first[1::2], axis=1)
+
+    total_copies = []
+    for d in range(1, sp_size):
+        copy = pltpu.make_async_remote_copy(
+            src_ref=totals.at[sp],
+            dst_ref=totals.at[sp],
+            send_sem=total_send.at[d],
+            recv_sem=total_recv.at[d],
+            **at_device(lax.rem(sp + d, sp_size), tp),
+        )
+        copy.start()
+        total_copies.append(copy)
+
+    loads[1].wait()
+
+    with phase("gelu"):
+
+        @pl.loop(0, chunks)
+        def _(i):
+            r = pl.multiple_of(i * CHUNK, CHUNK)
+            lifted[pl.ds(r, CHUNK), :] = jax.nn.gelu(
+                out_gate_ref[pl.ds(r, CHUNK), :].astype(jnp.float32)
+            )
+
+    for load in loads[9:12]:
+        load.wait()
+    with phase("totals"):
+        for copy in total_copies:
+            copy.wait()
+
+    entering = jnp.zeros((1, channels), jnp.float32)
+    for k in range(sp_size):
+        part = totals[k]
+        after = part[0:1] * entering + part[1:2]
+        entering = jnp.where(k < sp, after, entering)
+    entering_rest = head_a * entering + head_h
+
+    both_rows = 2 * rows_dev
+
+    def fill_branch(side):
+        for q in range(both_rows // CHUNK):
+            r = pl.multiple_of(side * both_rows + q * CHUNK, CHUNK)
+            at = pl.ds(r, CHUNK)
+            before = entering_rest
+            if q == 0:
+                before = jnp.where(side == 0, entering, entering_rest)
+            state = local[at, :] + running[at, :] * before
+            branch[at, :] = (lifted[at, :] * state).astype(jnp.bfloat16)
+
+    def project(side, target):
+        fill_branch(side)
+        given = branch[pl.ds(pl.multiple_of(side * both_rows, both_rows), both_rows), :]
+        for n in range(steps):
+            cols = slice(n * step, (n + 1) * step)
+            product = jnp.dot(given, weight_ref[:, cols], preferred_element_type=jnp.float32)
+            target[0, :, cols] = product[:rows_dev]
+            target[1, :, cols] = product[rows_dev:]
+
+    def pair_copy(k, n):
+        return pltpu.make_async_remote_copy(
+            src_ref=send_pair.at[k, n],
+            dst_ref=recv_pair.at[k, n],
+            send_sem=pair_send.at[k, n],
+            recv_sem=pair_recv.at[k, n],
+            **at_device(sp, partner),
+        )
+
+    def send_partner(k, held):
+        for n in range(steps):
+            cols = slice(n * step, (n + 1) * step)
+            send_pair[k, n] = held[1 - core, :, cols].astype(jnp.bfloat16)
+            pair_copy(k, n).start()
+
+    with phase("project"):
+        project(other, across)
+        send_partner(0, across)
+        project(far, along)
+        send_partner(1, along)
+
+    def far_copy(q):
+        return pltpu.make_async_remote_copy(
+            src_ref=send_far.at[pl.ds(q * piece, piece)],
+            dst_ref=recv_far.at[pl.ds(q * piece, piece)],
+            send_sem=far_send.at[q],
+            recv_sem=far_recv.at[q],
+            **at_device(sp, across_tp),
+        )
+
+    with phase("far_send"):
+        for n in range(steps):
+            pair_copy(0, n).wait_recv()
+        for q in range(pieces):
+            at = slice(q * piece, (q + 1) * piece)
+            for n in range(steps):
+                cols = slice(n * step, (n + 1) * step)
+                sum_far = across[core, at, cols] + recv_pair[0, n, at, :].astype(jnp.float32)
+                send_far[at, cols] = sum_far.astype(jnp.bfloat16)
+            far_copy(q).start()
+    for n in range(steps):
+        cols = slice(n * step, (n + 1) * step)
+        pair_copy(1, n).wait_recv()
+        summed[:, cols] = (
+            along[core, :, cols]
+            + resid_ref[:, cols].astype(jnp.float32)
+            + recv_pair[1, n].astype(jnp.float32)
+        )
+
     slot_row = lax.broadcasted_iota(jnp.int32, (capacity, rows_dev), 0)
-
     expert_row = lax.broadcasted_iota(jnp.int32, (sp_size, rows_dev), 0)
     earlier = lax.broadcasted_iota(jnp.int32, (rows_dev, rows_dev), 0) < lax.broadcasted_iota(
         jnp.int32, (rows_dev, rows_dev), 1
     )
     earlier = jnp.where(earlier, 1.0, 0.0).astype(jnp.bfloat16)
 
-    def rank_block(block):
+    loads[7].wait()
+
+    @pl.loop(0, tp_size)
+    def _(block):
         chosen = routes_ref[block]
         hits = jnp.zeros((sp_size, rows_dev), jnp.float32)
         for k in range(picks):
             hits = hits + jnp.where(expert_row == chosen[k : k + 1], 1.0, 0.0)
-        ranks[block] = jnp.dot(
-            hits.astype(jnp.bfloat16), earlier, preferred_element_type=jnp.float32
-        )
+        ranks[block] = jnp.dot(hits.astype(jnp.bfloat16), earlier, preferred_element_type=jnp.float32)
 
     def selector(block, expert, values):
         chosen = routes_ref[block]
@@ -465,42 +771,90 @@
         rank = ranks[block, pl.ds(expert, 1), :].astype(jnp.int32)
         return jnp.where(rank == slot_row, value, 0.0)
 
-    def packed(expert):
-        ones = jnp.ones((picks, rows_dev), jnp.float32)
-        choose = selector(tp, expert, ones).astype(jnp.bfloat16)
-        return jnp.dot(choose, normed_ref[...], preferred_element_type=jnp.float32).astype(
-            jnp.bfloat16
-        )
-
     def slot_rows(block):
         return pl.ds(pl.multiple_of(block * capacity, capacity), capacity)
 
-    def source_of(d):
-        return lax.rem(sp - d + sp_size, sp_size)
-
-    def far_tp(j):
-        return lax.rem(far - j + far_size, far_size) * 2 + core
-
-    def weight_copy(u):
+    unit = jnp.ones((picks, rows_dev), jnp.float32)
+
+    @pl.loop(0, sp_size)
+    def _(d):
+        choose[slot_rows(d), :] = selector(tp, flipped(d), unit).astype(jnp.bfloat16)
+
+    @pl.loop(0, half)
+    def _(d):
+        choose_other[slot_rows(d), :] = selector(across_tp, flipped(d), unit).astype(jnp.bfloat16)
+
+    with phase("weights"):
+        for u in range(1, tp_size):
+            weight_copy(u).wait_recv()
+
+    with phase("mixers"):
+
+        @pl.loop(0, tp_size)
+        def _(block):
+            weight = pair_weights[block]
+            coarse = weight.astype(jnp.bfloat16).astype(jnp.float32)
+            for n, values in enumerate((coarse, weight - coarse)):
+                picked = [selector(block, e, values) for e in range(sp_size)]
+                mixers[block, n] = jnp.concatenate(picked, axis=0).T.astype(jnp.bfloat16)
+
+    def cross_copy(q):
         return pltpu.make_async_remote_copy(
-            src_ref=pair_weight_ref,
-            dst_ref=pair_weights.at[tp],
-            send_sem=weight_send.at[u],
-            recv_sem=weight_recv.at[u],
-            **at_device(sp, lax.rem(tp + u, tp_size)),
-        )
+            src_ref=normed_ref.at[pl.ds(q * piece, piece)],
+            dst_ref=other_normed.at[pl.ds(q * piece, piece)],
+            send_sem=cross_send.at[q],
+            recv_sem=cross_recv.at[q],
+            **at_device(sp, across_tp),
+        )
+
+    with phase("norm"):
+        for q in range(pieces):
+            at = slice(q * piece, (q + 1) * piece)
+            far_copy(q).wait_recv()
+            squares = jnp.zeros((piece, 1), jnp.float32)
+            for n in range(steps):
+                cols = slice(n * step, (n + 1) * step)
+                stream = (summed[at, cols] + recv_far[at, cols].astype(jnp.float32)).astype(jnp.bfloat16)
+                stream_ref[at, cols] = stream
+                wide = stream.astype(jnp.float32)
+                squares = squares + jnp.sum(wide * wide, axis=1, keepdims=True)
+            norm = lax.rsqrt(squares * (1.0 / width) + EPSILON)
+            for n in range(steps):
+                cols = slice(n * step, (n + 1) * step)
+                wide = stream_ref[at, cols].astype(jnp.float32)
+                normed_ref[at, cols] = (wide * norm * gain_ref[0:1, cols]).astype(jnp.bfloat16)
+            cross_copy(q).start()
 
     def out_copy(d):
         return pltpu.make_async_remote_copy(
-            src_ref=outgoing.at[d],
+            src_ref=outgoing.at[slot_rows(d)],
             dst_ref=rows.at[sp, slot_rows(tp)],
             send_sem=out_send.at[d],
             recv_sem=out_recv.at[d],
-            **at_device(lax.rem(sp + d, sp_size), tp),
+            **at_device(flipped(d), tp),
+        )
+
+    def near_copy(d):
+        return pltpu.make_async_remote_copy(
+            src_ref=outgoing_other.at[slot_rows(d)],
+            dst_ref=rows.at[sp, slot_rows(across_tp)],
+            send_sem=near_send.at[d],
+            recv_sem=near_recv.at[d],
+            **at_device(flipped(d), tp),
+        )
+
+    def row_far(d):
+        place = rows.at[flipped(d), slot_rows(tp)]
+        return pltpu.make_async_remote_copy(
+            src_ref=place,
+            dst_ref=place,
+            send_sem=row_far_send.at[d],
+            recv_sem=row_far_recv.at[d],
+            **at_device(sp, across_tp),
         )
 
     def row_pair(d, j):
-        place = rows.at[source_of(d), slot_rows(far_tp(j))]
+        place = rows.at[flipped(d), slot_rows(across_tp if j else tp)]
         return pltpu.make_async_remote_copy(
             src_ref=place,
             dst_ref=place,
@@ -509,18 +863,18 @@
             **at_device(sp, partner),
         )
 
-    def row_far(d, j):
-        place = rows.at[source_of(d), slot_rows(tp)]
+    def act_far(d):
+        place = active.at[flipped(d), tp]
         return pltpu.make_async_remote_copy(
             src_ref=place,
             dst_ref=place,
-            send_sem=row_far_send.at[d, j],
-            recv_sem=row_far_recv.at[d, j],
-            **at_device(sp, lax.rem(far + j, far_size) * 2 + core),
+            send_sem=act_far_send.at[d],
+            recv_sem=act_far_recv.at[d],
+            **at_device(sp, across_tp),
         )
 
     def act_pair(d, j):
-        place = active.at[source_of(d), far_tp(j)]
+        place = active.at[flipped(d), across_tp if j else tp]
         return pltpu.make_async_remote_copy(
             src_ref=place,
             dst_ref=place,
@@ -529,24 +883,16 @@
             **at_device(sp, partner),
         )
 
-    def act_far(d, j):
-        place = active.at[source_of(d), tp]
-        return pltpu.make_async_remote_copy(
-            src_ref=place,
-            dst_ref=place,
-            send_sem=act_far_send.at[d, j],
-            recv_sem=act_far_recv.at[d, j],
-            **at_device(sp, lax.rem(far + j, far_size) * 2 + core),
-        )
-
     def back_copy(d):
         return pltpu.make_async_remote_copy(
             src_ref=result.at[d],
             dst_ref=returned.at[sp],
             send_sem=back_send.at[d],
             recv_sem=back_recv.at[d],
-            **at_device(source_of(d), tp),
-        )
+            **at_device(flipped(d), tp),
+        )
+
+    mates = (across_tp, other * 2 + 1 - core, partner)
 
     def blend_copy(u):
         return pltpu.make_async_remote_copy(
@@ -554,79 +900,103 @@
             dst_ref=gathered.at[tp],
             send_sem=blend_send.at[u],
             recv_sem=blend_recv.at[u],
-            **at_device(sp, lax.rem(tp + u, tp_size)),
-        )
-
-    rank_block(tp)
-    rows[sp, slot_rows(tp), :] = packed(sp)
-    pair_weights[tp] = pair_weight_ref[...]
-    pl.semaphore_wait(barrier, sp_size - 1 + tp_size - 1)
-    for j in range(1, far_size):
-        row_far(0, j).start()
-    row_pair(0, 0).start()
-
-    @pl.loop(1, sp_size)
-    def _(d):
-        outgoing[d] = packed(lax.rem(sp + d, sp_size))
-        out_copy(d).start()
-
-    for u in range(1, tp_size):
-        weight_copy(u).start()
-
-    for load in loads:
+            **at_device(sp, mates[u]),
+        )
+
+    pack_rows = half * capacity
+
+    def pack(chooser, given, first_slot, target, first_row):
+        picked = chooser[first_slot : first_slot + pack_rows, :]
+        for n in range(steps):
+            cols = slice(n * step, (n + 1) * step)
+            target[first_row : first_row + pack_rows, cols] = jnp.dot(
+                picked, given[:, cols], preferred_element_type=jnp.float32
+            ).astype(jnp.bfloat16)
+
+    with phase("pack"):
+        pack(choose, normed_ref, pack_rows, outgoing, pack_rows)
+        for d in range(half, sp_size):
+            out_copy(d).start()
+        pack(choose, normed_ref, 0, outgoing, 0)
+        for d in range(1, half):
+            out_copy(d).start()
+        rows[sp, slot_rows(tp), :] = outgoing[0:capacity, :]
+        row_pair(0, 0).start()
+    with phase("cross"):
+        for q in range(pieces):
+            cross_copy(q).wait_recv()
+    with phase("pack_other"):
+        pack(choose_other, other_normed, 0, outgoing_other, 0)
+        for d in range(1, half):
+            near_copy(d).start()
+        rows[sp, slot_rows(across_tp), :] = outgoing_other[0:capacity, :]
+        row_pair(0, 1).start()
+
+    for load in loads[12:]:
         load.wait()
 
+    def is_near(i):
+        return lax.rem(i, 2)
+
+    def group(i):
+        near = lax.rem(i, 2)
+        return near * lax.rem((i + 1) // 2, half) + (1 - near) * (half + i // 2)
+
     @pl.loop(0, sp_size + 4)
-    def _(step):
-        @pl.when((step > 0) & (step < sp_size))
+    def _(s):
+        @pl.when((s < sp_size) & (is_near(s) == 0))
         def _():
-            out_copy(step).wait_recv()
-            for j in range(1, far_size):
-                row_far(step, j).start()
-            row_pair(step, 0).start()
-
-        @pl.when((step >= 2) & (step < sp_size + 2))
+            d = group(s)
+            with phase("w_out"):
+                out_copy(d).wait_recv()
+            row_far(d).start()
+            row_pair(d, 0).start()
+
+        @pl.when((s < sp_size - 1) & (is_near(s) == 1))
         def _():
-            d = step - 2
-            for j in range(far_size):
-                row_pair(d, j).wait_recv()
-            source = source_of(d)
+            d = group(s)
+            with phase("w_near"):
+                out_copy(d).wait_recv()
+                row_pair(d, 0).start()
+                near_copy(d).wait_recv()
+                row_pair(d, 1).start()
+
+        @pl.when((s >= 2) & (s < sp_size + 2))
+        def _():
+            d = group(s - 2)
+            with phase("w_rowpair"):
+                row_pair(d, 0).wait_recv()
+                row_pair(d, 1).wait_recv()
+            source = flipped(d)
             given = rows[source]
             gated = jnp.dot(given, gate[...], preferred_element_type=jnp.float32)
             upward = jnp.dot(given, up[...], preferred_element_type=jnp.float32)
             active[source, tp] = (jax.nn.silu(gated) * upward).astype(jnp.bfloat16)
-            for j in range(1, far_size):
-                act_far(d, j).start()
+            act_far(d).start()
             act_pair(d, 0).start()
 
-        @pl.when((step >= 3) & (step < sp_size + 3))
+        @pl.when((s >= 3) & (s < sp_size + 3))
         def _():
-            for j in range(1, far_size):
-                act_far(step - 3, j).wait_recv()
-                act_pair(step - 3, j).start()
-
-        @pl.when((step >= 1) & (step < sp_size + 1))
+            d = group(s - 3)
+            with phase("w_actfar"):
+                act_far(d).wait_recv()
+            act_pair(d, 1).start()
+
+        @pl.when((s >= 1) & (s < sp_size + 1) & (is_near(s) == 1))
         def _():
-            for j in range(1, far_size):
-                row_far(step - 1, j).wait_recv()
-                row_pair(step - 1, j).start()
-
-        for u in range(1, tp_size):
-
-            @pl.when(step == 3)
-            def _(u=u):
-                weight_copy(u).wait_recv()
-                rank_block(lax.rem(tp + u, tp_size))
-
-        @pl.when(step >= 4)
+            d = group(s - 1)
+            with phase("w_rowfar"):
+                row_far(d).wait_recv()
+            row_pair(d, 1).start()
+
+        @pl.when(s >= 4)
         def _():
-            d = step - 4
-            for j in range(far_size):
-                act_pair(d, j).wait_recv()
-            source = source_of(d)
-            total = jnp.dot(
-                active[source, 0], down[0:hidden, :], preferred_element_type=jnp.float32
-            )
+            d = group(s - 4)
+            with phase("w_actpair"):
+                act_pair(d, 0).wait_recv()
+                act_pair(d, 1).wait_recv()
+            source = flipped(d)
+            total = jnp.dot(active[source, 0], down[0:hidden, :], preferred_element_type=jnp.float32)
             for t in range(1, tp_size):
                 total = total + jnp.dot(
                     active[source, t],
@@ -643,17 +1013,11 @@
             def _():
                 back_copy(d).start()
 
-            @pl.when(d < tp_size)
-            def _():
-                weight = pair_weights[d]
-                coarse = weight.astype(jnp.bfloat16).astype(jnp.float32)
-                for n, values in enumerate((coarse, weight - coarse)):
-                    picked = [selector(d, e, values) for e in range(sp_size)]
-                    mixers[d, n] = jnp.concatenate(picked, axis=0).T.astype(jnp.bfloat16)
-
-    @pl.loop(1, sp_size)
-    def _(d):
-        back_copy(d).wait_recv()
+    with phase("w_back"):
+
+        @pl.loop(1, sp_size)
+        def _(d):
+            back_copy(d).wait_recv()
 
     def blended(block):
         part = returned[:, slot_rows(block), :].reshape(sp_size * capacity, columns)
@@ -661,21 +1025,29 @@
         total = total + jnp.dot(mixers[block, 1], part, preferred_element_type=jnp.float32)
         return total.astype(jnp.bfloat16)
 
-    for u in [*range(2, tp_size), 1]:
-        blend[u] = blended(lax.rem(tp + u, tp_size))
-        blend_copy(u).start()
-
-    gathered[tp] = blended(tp)
-    for u in range(1, tp_size):
-        blend_copy(u).wait_recv()
+    with phase("blend"):
+        for u, mate in enumerate(mates):
+            blend[u] = blended(mate)
+            blend_copy(u).start()
+        gathered[tp] = blended(tp)
+    with phase("w_blend"):
+        for u in range(tp_size - 1):
+            blend_copy(u).wait_recv()
     for t in range(tp_size):
         cols = slice(t * columns, (t + 1) * columns)
         out_ref[:, cols] = (
             stream_ref[:, cols].astype(jnp.float32) + gathered[t].astype(jnp.float32)
         ).astype(jnp.bfloat16)
 
+    for k in range(2):
+        for n in range(steps):
+            pair_copy(k, n).wait_send()
+    for q in range(pieces):
+        far_copy(q).wait_send()
+        cross_copy(q).wait_send()
     for u in range(1, tp_size):
         weight_copy(u).wait_send()
+    for u in range(tp_size - 1):
         blend_copy(u).wait_send()
 
     @pl.loop(1, sp_size)
@@ -683,67 +1055,147 @@
         out_copy(d).wait_send()
         back_copy(d).wait_send()
 
+    @pl.loop(1, half)
+    def _(d):
+        near_copy(d).wait_send()
+
+    @pl.loop(half, sp_size)
+    def _(d):
+        row_far(d).wait_send()
+
     @pl.loop(0, sp_size)
     def _(d):
-        for j in range(far_size):
+        act_far(d).wait_send()
+        for j in range(2):
             row_pair(d, j).wait_send()
             act_pair(d, j).wait_send()
-        for j in range(1, far_size):
-            row_far(d, j).wait_send()
-            act_far(d, j).wait_send()
-
-
-def routed_experts(
-    normed, stream, routes, expert_pair_weight, gate_weight, up_weight, down_weight, capacity
+
+
+def fused_layer(
+    resid,
+    recurrent_input,
+    recurrent_out_gate,
+    filter_weight,
+    recurrence_gate_matrix,
+    input_gate_matrix,
+    channel_decay_raw,
+    token_decay_boost,
+    output_projection_weight,
+    expert_norm_gain,
+    routes,
+    expert_pair_weight,
+    gate_weight,
+    up_weight,
+    down_weight,
+    capacity,
 ):
     sp_size, tp_size = lax.axis_size("sp"), lax.axis_size("tp")
-    rows_dev, width = normed.shape
+    tokens, channels = recurrent_input.shape
+    rows_dev, width = resid.shape
     hidden, columns = gate_weight.shape[2], down_weight.shape[2]
-    by_block = routes.reshape(tp_size, rows_dev, -1).swapaxes(1, 2)
-    pair_weight = jnp.pad(expert_pair_weight.T, ((0, TILE - expert_pair_weight.shape[1]), (0, 0)))
-    vmem = pl.BlockSpec(memory_space=pltpu.VMEM)
-    anywhere = pl.BlockSpec(memory_space=pl.ANY)
-    far_size = tp_size // 2
+    step = 512 if width % 512 == 0 else width
+    steps = width // step
+    pieces = 4 if rows_dev % (4 * RIM) == 0 else 1
+    half = sp_size // 2
+    slots_all = tp_size * capacity
+    narrow = (
+        recurrent_input,
+        recurrent_out_gate,
+        filter_weight,
+        recurrence_gate_matrix,
+        input_gate_matrix,
+        channel_decay_raw.reshape(1, channels),
+        token_decay_boost,
+        routes.reshape(tp_size, rows_dev, -1).swapaxes(1, 2),
+        expert_pair_weight.T,
+        output_projection_weight,
+        resid,
+        expert_norm_gain.reshape(1, width),
+    )
+    operands = (*narrow, gate_weight, up_weight, down_weight)
+    dma = pltpu.SemaphoreType.DMA
 
     def buffer(*shape):
         return pltpu.VMEM(shape, jnp.bfloat16)
 
-    slots_all = tp_size * capacity
-    dma = pltpu.SemaphoreType.DMA
+    def wide(*shape):
+        return pltpu.VMEM(shape, jnp.float32)
+
     return pl.pallas_call(
-        functools.partial(experts_kernel, sp_size, tp_size, capacity),
+        functools.partial(layer_kernel, sp_size, tp_size, capacity),
         out_shape=jax.ShapeDtypeStruct((rows_dev, width), jnp.bfloat16),
-        in_specs=[vmem] * 4 + [anywhere] * 3,
-        out_specs=vmem,
+        in_specs=[pl.BlockSpec(memory_space=pltpu.HBM)] * len(operands),
+        out_specs=pl.BlockSpec(memory_space=pltpu.VMEM),
         scratch_shapes=[
+            *[pltpu.VMEM(operand.shape, operand.dtype) for operand in narrow],
             buffer(*gate_weight.shape[1:]),
             buffer(*up_weight.shape[1:]),
             buffer(*down_weight.shape[1:]),
-            buffer(sp_size, capacity, width),
+            buffer(channels // LANES, LANES, 2 * LANES),
+            wide(tokens + TILE, channels),
+            buffer(RIM, channels),
+            wide(tokens, channels),
+            wide(tokens, channels),
+            wide(tokens, channels),
+            buffer(tokens, channels),
+            wide(sp_size, TILE, channels),
+            wide(2, rows_dev, width),
+            wide(2, rows_dev, width),
+            buffer(2, steps, rows_dev, step),
+            buffer(2, steps, rows_dev, step),
+            buffer(rows_dev, width),
+            buffer(rows_dev, width),
+            wide(rows_dev, width),
+            buffer(rows_dev, width),
+            buffer(rows_dev, width),
+            buffer(rows_dev, width),
+            wide(TILE, rows_dev),
+            wide(tp_size, TILE, rows_dev),
+            wide(tp_size, sp_size, rows_dev),
+            buffer(sp_size * capacity, rows_dev),
+            buffer(half * capacity, rows_dev),
+            buffer(tp_size, 2, rows_dev, sp_size * capacity),
+            buffer(sp_size * capacity, width),
+            buffer(half * capacity, width),
             buffer(sp_size, slots_all, width),
             buffer(sp_size, tp_size, slots_all, hidden),
             buffer(sp_size, slots_all, columns),
             buffer(sp_size, slots_all, columns),
+            buffer(tp_size - 1, rows_dev, columns),
             buffer(tp_size, rows_dev, columns),
-            buffer(tp_size, rows_dev, columns),
-            pltpu.VMEM((tp_size, TILE, rows_dev), jnp.float32),
-            pltpu.VMEM((tp_size, sp_size, rows_dev), jnp.float32),
-            buffer(tp_size, 2, rows_dev, sp_size * capacity),
-            dma((3,)),
+            dma((len(operands),)),
+            dma((2,)),
+            dma((sp_size,)),
+            dma((sp_size,)),
+            dma((2, steps)),
+            dma((2, steps)),
+            dma((pieces,)),
+            dma((pieces,)),
+            dma((pieces,)),
+            dma((pieces,)),
             dma((tp_size,)),
             dma((tp_size,)),
             dma((sp_size,)),
             dma((sp_size,)),
-            *[dma((sp_size, far_size))] * 8,
+            dma((half,)),
+            dma((half,)),
             dma((sp_size,)),
             dma((sp_size,)),
-            dma((tp_size,)),
-            dma((tp_size,)),
+            dma((sp_size, 2)),
+            dma((sp_size, 2)),
+            dma((sp_size,)),
+            dma((sp_size,)),
+            dma((sp_size, 2)),
+            dma((sp_size, 2)),
+            dma((sp_size,)),
+            dma((sp_size,)),
+            dma((tp_size - 1,)),
+            dma((tp_size - 1,)),
         ],
         compiler_params=pltpu.CompilerParams(
             collective_id=1, has_side_effects=True, vmem_limit_bytes=67043328
         ),
-    )(normed, stream, by_block, pair_weight, gate_weight, up_weight, down_weight)
+    )(*operands)
 
 
 def body(
@@ -764,6 +1216,29 @@
     down_weight,
 ):
     tp_size = lax.axis_size("tp")
+    experts = lax.axis_size("sp")
+    rows_dev, model_width = resid.shape
+    capacity = max(2, 3 * rows_dev // experts)
+    fits = capacity % RIM == 0 and rows_dev % LANES == 0
+    if fits and tp_size == 4 and experts >= 4 and experts & (experts - 1) == 0:
+        return fused_layer(
+            resid,
+            recurrent_input,
+            recurrent_out_gate,
+            filter_weight,
+            recurrence_gate_matrix,
+            input_gate_matrix,
+            channel_decay_raw,
+            token_decay_boost,
+            output_projection_weight,
+            expert_norm_gain,
+            routes,
+            expert_pair_weight,
+            gate_weight,
+            up_weight,
+            down_weight,
+            capacity,
+        )
     stream, normed = recurrence(
         resid,
         recurrent_input,
@@ -777,21 +1252,6 @@
         expert_norm_gain,
     )
     stream_wide = stream.astype(jnp.float32)
-    rows_dev = stream.shape[0]
-    model_width = normed.shape[1]
-    experts = lax.axis_size("sp")
-    capacity = max(2, 3 * rows_dev // experts)
-    if capacity % RIM == 0 and rows_dev % LANES == 0 and tp_size <= experts:
-        return routed_experts(
-            normed,
-            stream,
-            routes,
-            expert_pair_weight,
-            gate_weight,
-            up_weight,
-            down_weight,
-            capacity,
-        )
     own_routes = lax.dynamic_slice_in_dim(routes, lax.axis_index("tp") * rows_dev, rows_dev, 0)
     own_flat, own_rank = slot_numbers(own_routes, experts)
     own_slots = own_flat * capacity + own_rank

time: 150 us -> 132 us (0.88); the launches traced: 149 us -> 132 us
  Pallas kernels: 145 us -> 130 us
    pallas_call x2 -> x1, Pallas kernels: 145 us -> 130 us  [fused_layer(): pl.pallas_call(functools.partial(layer_kernel, sp_size, tp_size, capacity...]
where the time goes in v1:
time: 132 us
  Pallas kernels  130 us (98%)
  local copies, waits for them, and re-layouts  1.88 us (1%)
    pallas_call x1, Pallas kernels, fused_layer(): pl.pallas_call(functools.partial(layer_kernel, sp_size, tp_size, capacity...  130 us

profile of v1, /device:TPU:0, one launch (start us, length us, event | category | flops | bytes accessed | tf_op | source)
XLA Modules:
  0.0 132.2 jit_solution(13481362633400908482)
XLA Ops:
  0.0 130.3 %shard_map.145 = bf16[128,2048]{1,0:T(8,128)(2,1)} custom-call(bf16[512,512]{1,0:T(8,128)(2,1)} %x_hbm.1, bf16[512,512]{1,0:T(8,128)(2,1)} %out_gate_hbm.1, f32[4,512]{1,0:T(4,128)} %taps_hbm.1, bf16[8,64,64]{2,1,0:T(8,128)(2,1)} %recur_map_hbm.1, bf16[8,64,64]{2,1,0:T(8,128)(2,1)} %input_map_hbm.1, f32[1,512]{1,0:T(1,128)} %bitcast.8, ...), custom_call_target="tpu_custom_call" | custom-call | tf_op jit(solution)/shard_map/pallas_call | solution.py:1124
  130.3 1.9 %copy.17 = bf16[128,2048]{1,0:T(8,128)(2,1)} copy(bf16[128,2048]{1,0:T(8,128)(2,1)} %shard_map.145) | data formatting | bytes 1048576

commit v2 on v1

--- a/solution.py
+++ b/solution.py
@@ -434,22 +434,29 @@
     stream_ref,
     normed_ref,
     other_normed,
+    mirrored,
     own_weights,
     pair_weights,
     ranks,
     choose,
     choose_other,
+    choose_mirror,
     mixers,
     outgoing,
     outgoing_other,
+    outgoing_mirror,
     rows,
     active,
     result,
     returned,
     blend,
     gathered,
+    gate_extra,
+    up_extra,
     load_sems,
     rim_sems,
+    extra_send,
+    extra_recv,
     total_send,
     total_recv,
     pair_send,
@@ -458,24 +465,30 @@
     far_recv,
     cross_send,
     cross_recv,
+    mirror_send,
+    mirror_recv,
+    route_sems,
     weight_send,
     weight_recv,
     out_send,
     out_recv,
     near_send,
     near_recv,
+    pass_send,
+    pass_recv,
     row_far_send,
     row_far_recv,
     row_pair_send,
     row_pair_recv,
-    act_far_send,
-    act_far_recv,
-    act_pair_send,
-    act_pair_recv,
-    back_send,
-    back_recv,
+    half_send,
+    half_recv,
+    half_pair_send,
+    half_pair_recv,
+    back_half_send,
+    back_half_recv,
     blend_send,
     blend_recv,
+    store_sems,
 ):
     sp, tp = lax.axis_index("sp"), lax.axis_index("tp")
     tokens, channels = x_ref.shape
@@ -489,6 +502,7 @@
     across_tp = other * 2 + core
     half = sp_size // 2
     steps, step = send_pair.shape[1], send_pair.shape[3]
+    kept = hidden - gate_extra.shape[1]
     pieces = far_send.shape[0]
     piece = rows_dev // pieces
 
@@ -507,7 +521,7 @@
         (input_map_hbm, input_map_ref),
         (decay_hbm, decay_ref),
         (boost_hbm, boost_ref),
-        (routes_hbm, routes_ref),
+        (routes_hbm, routes_ref.at[0:tp_size]),
         (pair_weight_hbm, pair_weight_ref),
         (weight_hbm, weight_ref),
         (resid_hbm, resid_ref),
@@ -570,6 +584,21 @@
     )
     rim_copy.start()
 
+    def extra_copy(n):
+        source, target = ((gate_hbm, gate_extra), (up_hbm, up_extra))[n]
+        return pltpu.make_async_remote_copy(
+            src_ref=source.at[0, :, kept:hidden],
+            dst_ref=target,
+            send_sem=extra_send.at[n],
+            recv_sem=extra_recv.at[n],
+            **at_device(sp, across_tp),
+        )
+
+    @pl.when(core == 0)
+    def _():
+        for n in range(2):
+            extra_copy(n).start()
+
     def weight_copy(u):
         return pltpu.make_async_remote_copy(
             src_ref=own_weights,
@@ -581,6 +610,15 @@
 
     for u in range(1, tp_size):
         weight_copy(u).start()
+    loads[7].wait()
+    route_copy = pltpu.make_async_remote_copy(
+        src_ref=routes_ref.at[tp],
+        dst_ref=routes_ref.at[tp_size],
+        send_sem=route_sems.at[0],
+        recv_sem=route_sems.at[1],
+        **at_device(flipped(half), tp),
+    )
+    route_copy.start()
     loads[6].wait()
     for load in loads[12:]:
         load.start()
@@ -688,7 +726,16 @@
             state = local[at, :] + running[at, :] * before
             branch[at, :] = (lifted[at, :] * state).astype(jnp.bfloat16)
 
-    def project(side, target):
+    def pair_copy(k, n):
+        return pltpu.make_async_remote_copy(
+            src_ref=send_pair.at[k, n],
+            dst_ref=recv_pair.at[k, n],
+            send_sem=pair_send.at[k, n],
+            recv_sem=pair_recv.at[k, n],
+            **at_device(sp, partner),
+        )
+
+    def project(side, target, k, send):
         fill_branch(side)
         given = branch[pl.ds(pl.multiple_of(side * both_rows, both_rows), both_rows), :]
         for n in range(steps):
@@ -696,27 +743,13 @@
             product = jnp.dot(given, weight_ref[:, cols], preferred_element_type=jnp.float32)
             target[0, :, cols] = product[:rows_dev]
             target[1, :, cols] = product[rows_dev:]
-
-    def pair_copy(k, n):
-        return pltpu.make_async_remote_copy(
-            src_ref=send_pair.at[k, n],
-            dst_ref=recv_pair.at[k, n],
-            send_sem=pair_send.at[k, n],
-            recv_sem=pair_recv.at[k, n],
-            **at_device(sp, partner),
-        )
-
-    def send_partner(k, held):
-        for n in range(steps):
-            cols = slice(n * step, (n + 1) * step)
-            send_pair[k, n] = held[1 - core, :, cols].astype(jnp.bfloat16)
-            pair_copy(k, n).start()
+            send_pair[k, n] = target[1 - core, :, cols].astype(jnp.bfloat16)
+            if send:
+                pair_copy(k, n).start()
 
     with phase("project"):
-        project(other, across)
-        send_partner(0, across)
-        project(far, along)
-        send_partner(1, along)
+        project(other, across, 0, True)
+        project(far, along, 1, False)
 
     def far_copy(q):
         return pltpu.make_async_remote_copy(
@@ -738,6 +771,8 @@
                 send_far[at, cols] = sum_far.astype(jnp.bfloat16)
             far_copy(q).start()
     for n in range(steps):
+        pair_copy(1, n).start()
+    for n in range(steps):
         cols = slice(n * step, (n + 1) * step)
         pair_copy(1, n).wait_recv()
         summed[:, cols] = (
@@ -753,9 +788,9 @@
     )
     earlier = jnp.where(earlier, 1.0, 0.0).astype(jnp.bfloat16)
 
-    loads[7].wait()
-
-    @pl.loop(0, tp_size)
+    route_copy.wait()
+
+    @pl.loop(0, tp_size + 1)
     def _(block):
         chosen = routes_ref[block]
         hits = jnp.zeros((sp_size, rows_dev), jnp.float32)
@@ -776,13 +811,12 @@
 
     unit = jnp.ones((picks, rows_dev), jnp.float32)
 
-    @pl.loop(0, sp_size)
-    def _(d):
-        choose[slot_rows(d), :] = selector(tp, flipped(d), unit).astype(jnp.bfloat16)
-
     @pl.loop(0, half)
     def _(d):
-        choose_other[slot_rows(d), :] = selector(across_tp, flipped(d), unit).astype(jnp.bfloat16)
+        expert = flipped(d)
+        choose[slot_rows(d), :] = selector(tp, expert, unit).astype(jnp.bfloat16)
+        choose_other[slot_rows(d), :] = selector(across_tp, expert, unit).astype(jnp.bfloat16)
+        choose_mirror[slot_rows(d), :] = selector(tp_size, expert, unit).astype(jnp.bfloat16)
 
     with phase("weights"):
         for u in range(1, tp_size):
@@ -805,6 +839,15 @@
             send_sem=cross_send.at[q],
             recv_sem=cross_recv.at[q],
             **at_device(sp, across_tp),
+        )
+
+    def mirror_copy(q):
+        return pltpu.make_async_remote_copy(
+            src_ref=normed_ref.at[pl.ds(q * piece, piece)],
+            dst_ref=mirrored.at[pl.ds(q * piece, piece)],
+            send_sem=mirror_send.at[q],
+            recv_sem=mirror_recv.at[q],
+            **at_device(flipped(half), tp),
         )
 
     with phase("norm"):
@@ -824,6 +867,7 @@
                 wide = stream_ref[at, cols].astype(jnp.float32)
                 normed_ref[at, cols] = (wide * norm * gain_ref[0:1, cols]).astype(jnp.bfloat16)
             cross_copy(q).start()
+            mirror_copy(q).start()
 
     def out_copy(d):
         return pltpu.make_async_remote_copy(
@@ -843,13 +887,22 @@
             **at_device(flipped(d), tp),
         )
 
+    def pass_copy(e):
+        return pltpu.make_async_remote_copy(
+            src_ref=outgoing_mirror.at[slot_rows(e)],
+            dst_ref=rows.at[flipped(half), slot_rows(tp)],
+            send_sem=pass_send.at[e],
+            recv_sem=pass_recv.at[e],
+            **at_device(flipped(e), tp),
+        )
+
     def row_far(d):
         place = rows.at[flipped(d), slot_rows(tp)]
         return pltpu.make_async_remote_copy(
             src_ref=place,
             dst_ref=place,
-            send_sem=row_far_send.at[d],
-            recv_sem=row_far_recv.at[d],
+            send_sem=row_far_send.at[d - half],
+            recv_sem=row_far_recv.at[d - half],
             **at_device(sp, across_tp),
         )
 
@@ -863,32 +916,51 @@
             **at_device(sp, partner),
         )
 
-    def act_far(d):
-        place = active.at[flipped(d), tp]
+    half_slots = 2 * capacity
+
+    def side_rows(side):
+        return pl.ds(pl.multiple_of(side * half_slots, half_slots), half_slots)
+
+    sides = (far, other)
+
+    def half_copy(d, h, end):
+        place = active.at[flipped(d), tp, side_rows(sides[h]), 0:end]
         return pltpu.make_async_remote_copy(
             src_ref=place,
             dst_ref=place,
-            send_sem=act_far_send.at[d],
-            recv_sem=act_far_recv.at[d],
+            send_sem=half_send.at[d, h],
+            recv_sem=half_recv.at[d, h],
             **at_device(sp, across_tp),
         )
 
-    def act_pair(d, j):
-        place = active.at[flipped(d), across_tp if j else tp]
+    def on_half(d, h, act):
+        @pl.when(core == 0)
+        def _():
+            act(half_copy(d, h, kept))
+
+        @pl.when(core == 1)
+        def _():
+            act(half_copy(d, h, hidden))
+
+    def half_start(d, h):
+        on_half(d, h, lambda copy: copy.start())
+
+    def half_pair(d, j, h):
+        place = active.at[flipped(d), across_tp if j else tp, side_rows(sides[h])]
         return pltpu.make_async_remote_copy(
             src_ref=place,
             dst_ref=place,
-            send_sem=act_pair_send.at[d, j],
-            recv_sem=act_pair_recv.at[d, j],
+            send_sem=half_pair_send.at[d, 2 * j + h],
+            recv_sem=half_pair_recv.at[d, 2 * j + h],
             **at_device(sp, partner),
         )
 
-    def back_copy(d):
+    def back_half(d, h):
         return pltpu.make_async_remote_copy(
-            src_ref=result.at[d],
-            dst_ref=returned.at[sp],
-            send_sem=back_send.at[d],
-            recv_sem=back_recv.at[d],
+            src_ref=result.at[d, side_rows(sides[h])],
+            dst_ref=returned.at[sp, side_rows(sides[h])],
+            send_sem=back_half_send.at[d, h],
+            recv_sem=back_half_recv.at[d, h],
             **at_device(flipped(d), tp),
         )
 
@@ -905,119 +977,206 @@
 
     pack_rows = half * capacity
 
-    def pack(chooser, given, first_slot, target, first_row):
-        picked = chooser[first_slot : first_slot + pack_rows, :]
+    def pack(chooser, given, target):
         for n in range(steps):
             cols = slice(n * step, (n + 1) * step)
-            target[first_row : first_row + pack_rows, cols] = jnp.dot(
-                picked, given[:, cols], preferred_element_type=jnp.float32
+            target[:, cols] = jnp.dot(
+                chooser[...], given[:, cols], preferred_element_type=jnp.float32
             ).astype(jnp.bfloat16)
 
+    def hidden_part(given, gate_part, up_part):
+        gated = jnp.dot(given, gate_part[...], preferred_element_type=jnp.float32)
+        upward = jnp.dot(given, up_part[...], preferred_element_type=jnp.float32)
+        return (jax.nn.silu(gated) * upward).astype(jnp.bfloat16)
+
+    def fill_hidden(d, h):
+        source = flipped(d)
+        at = side_rows(sides[h])
+        active[source, tp, at, :] = hidden_part(rows[source, at, :], gate, up)
+        half_pair(d, 0, h).start()
+
+    def fill_extra(d, h):
+        source = flipped(d)
+        at = side_rows(sides[h])
+
+        @pl.when(core == 0)
+        def _():
+            active[source, across_tp, at, kept:hidden] = hidden_part(
+                rows[source, at, :], gate_extra, up_extra
+            )
+
+    def first(d):
+        with phase("w_first"):
+            row_pair(d, 0).wait_recv()
+        fill_hidden(d, 0)
+        half_start(d, 0)
+        fill_extra(d, 0)
+
+    def second(d):
+        with phase("w_second"):
+            row_pair(d, 1).wait_recv()
+        fill_hidden(d, 1)
+        fill_extra(d, 1)
+
+    def relay(d, h):
+        with phase("w_relay"):
+            on_half(d, h, lambda copy: copy.wait_recv())
+        half_pair(d, 1, 1 - h).start()
+
+    def down_side(d, h):
+        with phase("w_down"):
+            half_pair(d, 0, h).wait_recv()
+            half_pair(d, 1, h).wait_recv()
+        source = flipped(d)
+        at = side_rows(sides[h])
+        total = jnp.dot(active[source, 0, at, :], down[0:hidden, :], preferred_element_type=jnp.float32)
+        for t in range(1, tp_size):
+            total = total + jnp.dot(
+                active[source, t, at, :],
+                down[t * hidden : (t + 1) * hidden, :],
+                preferred_element_type=jnp.float32,
+            )
+        made = total.astype(jnp.bfloat16)
+        result[d, at, :] = made
+
+        @pl.when(d == 0)
+        def _():
+            returned[sp, at, :] = made
+
+        @pl.when(d > 0)
+        def _():
+            back_half(d, h).start()
+
+    def near_first(d):
+        with phase("w_own"):
+
+            @pl.when(d > 0)
+            def _():
+                out_copy(d).wait_recv()
+                row_pair(d, 0).start()
+
+        first(d)
+
+    def near_arrived(d):
+        with phase("w_near"):
+
+            @pl.when(d > 0)
+            def _():
+                near_copy(d).wait_recv()
+                row_pair(d, 1).start()
+
     with phase("pack"):
-        pack(choose, normed_ref, pack_rows, outgoing, pack_rows)
-        for d in range(half, sp_size):
-            out_copy(d).start()
-        pack(choose, normed_ref, 0, outgoing, 0)
-        for d in range(1, half):
-            out_copy(d).start()
+        pack(choose, normed_ref, outgoing)
+        out_copy(1).start()
         rows[sp, slot_rows(tp), :] = outgoing[0:capacity, :]
         row_pair(0, 0).start()
+    for load in loads[12:]:
+        load.wait()
+
+    @pl.when(core == 0)
+    def _():
+        for n in range(2):
+            extra_copy(n).wait_recv()
+
+    @pl.loop(0, half // 2)
+    def _(d):
+        near_first(d)
+
     with phase("cross"):
         for q in range(pieces):
             cross_copy(q).wait_recv()
     with phase("pack_other"):
-        pack(choose_other, other_normed, 0, outgoing_other, 0)
-        for d in range(1, half):
-            near_copy(d).start()
+        pack(choose_other, other_normed, outgoing_other)
         rows[sp, slot_rows(across_tp), :] = outgoing_other[0:capacity, :]
         row_pair(0, 1).start()
-
-    for load in loads[12:]:
-        load.wait()
-
-    def is_near(i):
-        return lax.rem(i, 2)
-
-    def group(i):
-        near = lax.rem(i, 2)
-        return near * lax.rem((i + 1) // 2, half) + (1 - near) * (half + i // 2)
-
-    @pl.loop(0, sp_size + 4)
+    with phase("mirror"):
+        for q in range(pieces):
+            mirror_copy(q).wait_recv()
+    with phase("pack_mirror"):
+        pack(choose_mirror, mirrored, outgoing_mirror)
+        for e in range(1, min(3, half)):
+            pass_copy(e).start()
+        near_copy(1).start()
+        rows[flipped(half), slot_rows(tp), :] = outgoing_mirror[0:capacity, :]
+        row_far(half).start()
+        row_pair(half, 0).start()
+
+    first(half)
+
+    @pl.loop(1, half + 1)
     def _(s):
-        @pl.when((s < sp_size) & (is_near(s) == 0))
+        d = half + s
+        near = s - 1
+
+        @pl.when(s < half)
         def _():
-            d = group(s)
-            with phase("w_out"):
-                out_copy(d).wait_recv()
+            with phase("w_pass"):
+                pass_copy(s).wait_recv()
             row_far(d).start()
             row_pair(d, 0).start()
 
-        @pl.when((s < sp_size - 1) & (is_near(s) == 1))
+        @pl.when(s + 2 < half)
         def _():
-            d = group(s)
-            with phase("w_near"):
-                out_copy(d).wait_recv()
-                row_pair(d, 0).start()
-                near_copy(d).wait_recv()
-                row_pair(d, 1).start()
-
-        @pl.when((s >= 2) & (s < sp_size + 2))
+            pass_copy(s + 2).start()
+
+        @pl.when(s + 1 < half)
         def _():
-            d = group(s - 2)
-            with phase("w_rowpair"):
-                row_pair(d, 0).wait_recv()
-                row_pair(d, 1).wait_recv()
-            source = flipped(d)
-            given = rows[source]
-            gated = jnp.dot(given, gate[...], preferred_element_type=jnp.float32)
-            upward = jnp.dot(given, up[...], preferred_element_type=jnp.float32)
-            active[source, tp] = (jax.nn.silu(gated) * upward).astype(jnp.bfloat16)
-            act_far(d).start()
-            act_pair(d, 0).start()
-
-        @pl.when((s >= 3) & (s < sp_size + 3))
+            out_copy(s + 1).start()
+            near_copy(s + 1).start()
+
+        with phase("w_rowfar"):
+            row_far(d - 1).wait_recv()
+        row_pair(d - 1, 1).start()
+
+        @pl.when(s >= 2)
         def _():
-            d = group(s - 3)
-            with phase("w_actfar"):
-                act_far(d).wait_recv()
-            act_pair(d, 1).start()
-
-        @pl.when((s >= 1) & (s < sp_size + 1) & (is_near(s) == 1))
+            relay(d - 2, 1)
+
+        @pl.when(s < half)
         def _():
-            d = group(s - 1)
-            with phase("w_rowfar"):
-                row_far(d).wait_recv()
-            row_pair(d, 1).start()
-
-        @pl.when(s >= 4)
+            first(d)
+
+        second(d - 1)
+        half_start(d - 1, 1)
+        relay(d - 1, 0)
+        near_arrived(near)
+
+        @pl.when(s >= 2)
         def _():
-            d = group(s - 4)
-            with phase("w_actpair"):
-                act_pair(d, 0).wait_recv()
-                act_pair(d, 1).wait_recv()
-            source = flipped(d)
-            total = jnp.dot(active[source, 0], down[0:hidden, :], preferred_element_type=jnp.float32)
-            for t in range(1, tp_size):
-                total = total + jnp.dot(
-                    active[source, t],
-                    down[t * hidden : (t + 1) * hidden, :],
-                    preferred_element_type=jnp.float32,
-                )
-            result[d] = total.astype(jnp.bfloat16)
-
-            @pl.when(d == 0)
-            def _():
-                returned[sp] = total.astype(jnp.bfloat16)
-
-            @pl.when(d > 0)
-            def _():
-                back_copy(d).start()
-
-    with phase("w_back"):
-
-        @pl.loop(1, sp_size)
-        def _(d):
-            back_copy(d).wait_recv()
+            down_side(d - 2, 0)
+
+        @pl.when(near >= half // 2)
+        def _():
+            near_first(near)
+
+        down_side(d - 1, 1)
+
+        second(near)
+
+        @pl.when(near < half // 2)
+        def _():
+            relay(near, 0)
+            down_side(near, 1)
+
+    for d in reversed(range(half)):
+        half_start(d, 1)
+
+    relay(sp_size - 1, 1)
+
+    @pl.loop(half // 2, half)
+    def _(d):
+        relay(d, 0)
+        down_side(d, 1)
+
+    down_side(sp_size - 1, 0)
+
+    @pl.loop(1, half)
+    def _(d):
+        relay(half - d, 1)
+
+    @pl.loop(1, half)
+    def _(d):
+        down_side(half - d, 0)
 
     def blended(block):
         part = returned[:, slot_rows(block), :].reshape(sp_size * capacity, columns)
@@ -1025,19 +1184,33 @@
         total = total + jnp.dot(mixers[block, 1], part, preferred_element_type=jnp.float32)
         return total.astype(jnp.bfloat16)
 
+    with phase("w_back"):
+
+        @pl.loop(1, sp_size)
+        def _(d):
+            back_half(d, 1).wait_recv()
+
     with phase("blend"):
-        for u, mate in enumerate(mates):
-            blend[u] = blended(mate)
+        for u in range(2):
+            blend[u] = blended(mates[u])
             blend_copy(u).start()
-        gathered[tp] = blended(tp)
-    with phase("w_blend"):
-        for u in range(tp_size - 1):
-            blend_copy(u).wait_recv()
-    for t in range(tp_size):
-        cols = slice(t * columns, (t + 1) * columns)
-        out_ref[:, cols] = (
+
+    relay(0, 1)
+    down_side(0, 0)
+
+    @pl.loop(1, sp_size)
+    def _(d):
+        back_half(d, 0).wait_recv()
+
+    blend[2] = blended(partner)
+    blend_copy(2).start()
+    gathered[tp] = blended(tp)
+    def finish(n, t):
+        cols = pl.ds(pl.multiple_of(t * columns, columns), columns)
+        normed_ref[:, cols] = (
             stream_ref[:, cols].astype(jnp.float32) + gathered[t].astype(jnp.float32)
         ).astype(jnp.bfloat16)
+        pltpu.make_async_copy(normed_ref.at[:, cols], out_ref.at[:, cols], store_sems.at[n]).start()
 
     for k in range(2):
         for n in range(steps):
@@ -1045,19 +1218,26 @@
     for q in range(pieces):
         far_copy(q).wait_send()
         cross_copy(q).wait_send()
+        mirror_copy(q).wait_send()
     for u in range(1, tp_size):
         weight_copy(u).wait_send()
-    for u in range(tp_size - 1):
-        blend_copy(u).wait_send()
+
+    @pl.when(core == 0)
+    def _():
+        for n in range(2):
+            extra_copy(n).wait_send()
+
+
+    @pl.loop(1, half)
+    def _(d):
+        out_copy(d).wait_send()
+        near_copy(d).wait_send()
+        pass_copy(d).wait_send()
 
     @pl.loop(1, sp_size)
     def _(d):
-        out_copy(d).wait_send()
-        back_copy(d).wait_send()
-
-    @pl.loop(1, half)
-    def _(d):
-        near_copy(d).wait_send()
+        for h in range(2):
+            back_half(d, h).wait_send()
 
     @pl.loop(half, sp_size)
     def _(d):
@@ -1065,10 +1245,22 @@
 
     @pl.loop(0, sp_size)
     def _(d):
-        act_far(d).wait_send()
-        for j in range(2):
-            row_pair(d, j).wait_send()
-            act_pair(d, j).wait_send()
+        for h in range(2):
+            row_pair(d, h).wait_send()
+            on_half(d, h, lambda copy: copy.wait_send())
+            for j in range(2):
+                half_pair(d, j, h).wait_send()
+
+    finish(0, tp)
+    for n, u in enumerate((2, 0, 1)):
+        with phase("w_blend"):
+            blend_copy(u).wait_recv()
+        finish(n + 1, mates[u])
+    for u in range(tp_size - 1):
+        blend_copy(u).wait_send()
+    for n, t in enumerate((tp, mates[2], mates[0], mates[1])):
+        cols = pl.ds(pl.multiple_of(t * columns, columns), columns)
+        pltpu.make_async_copy(normed_ref.at[:, cols], out_ref.at[:, cols], store_sems.at[n]).wait()
 
 
 def fused_layer(
@@ -1125,9 +1317,11 @@
         functools.partial(layer_kernel, sp_size, tp_size, capacity),
         out_shape=jax.ShapeDtypeStruct((rows_dev, width), jnp.bfloat16),
         in_specs=[pl.BlockSpec(memory_space=pltpu.HBM)] * len(operands),
-        out_specs=pl.BlockSpec(memory_space=pltpu.VMEM),
+        out_specs=pl.BlockSpec(memory_space=pltpu.HBM),
         scratch_shapes=[
-            *[pltpu.VMEM(operand.shape, operand.dtype) for operand in narrow],
+            *[pltpu.VMEM(operand.shape, operand.dtype) for operand in narrow[:7]],
+            pltpu.VMEM((tp_size + 1, *narrow[7].shape[1:]), narrow[7].dtype),
+            *[pltpu.VMEM(operand.shape, operand.dtype) for operand in narrow[8:]],
             buffer(*gate_weight.shape[1:]),
             buffer(*up_weight.shape[1:]),
             buffer(*down_weight.shape[1:]),
@@ -1149,51 +1343,45 @@
             buffer(rows_dev, width),
             buffer(rows_dev, width),
             buffer(rows_dev, width),
+            buffer(rows_dev, width),
             wide(TILE, rows_dev),
             wide(tp_size, TILE, rows_dev),
-            wide(tp_size, sp_size, rows_dev),
-            buffer(sp_size * capacity, rows_dev),
-            buffer(half * capacity, rows_dev),
+            wide(tp_size + 1, sp_size, rows_dev),
+            *[buffer(half * capacity, rows_dev)] * 3,
             buffer(tp_size, 2, rows_dev, sp_size * capacity),
-            buffer(sp_size * capacity, width),
-            buffer(half * capacity, width),
+            *[buffer(half * capacity, width)] * 3,
             buffer(sp_size, slots_all, width),
             buffer(sp_size, tp_size, slots_all, hidden),
             buffer(sp_size, slots_all, columns),
             buffer(sp_size, slots_all, columns),
             buffer(tp_size - 1, rows_dev, columns),
             buffer(tp_size, rows_dev, columns),
+            buffer(width, LANES),
+            buffer(width, LANES),
             dma((len(operands),)),
+            dma((2,)),
+            dma((2,)),
             dma((2,)),
             dma((sp_size,)),
             dma((sp_size,)),
             dma((2, steps)),
             dma((2, steps)),
-            dma((pieces,)),
-            dma((pieces,)),
-            dma((pieces,)),
-            dma((pieces,)),
+            *[dma((pieces,))] * 6,
+            dma((2,)),
             dma((tp_size,)),
             dma((tp_size,)),
-            dma((sp_size,)),
-            dma((sp_size,)),
-            dma((half,)),
-            dma((half,)),
-            dma((sp_size,)),
-            dma((sp_size,)),
+            *[dma((half,))] * 8,
+            *[dma((sp_size, 2))] * 4,
+            dma((sp_size, 4)),
+            dma((sp_size, 4)),
             dma((sp_size, 2)),
             dma((sp_size, 2)),
-            dma((sp_size,)),
-            dma((sp_size,)),
-            dma((sp_size, 2)),
-            dma((sp_size, 2)),
-            dma((sp_size,)),
-            dma((sp_size,)),
             dma((tp_size - 1,)),
             dma((tp_size - 1,)),
+            dma((tp_size,)),
         ],
         compiler_params=pltpu.CompilerParams(
-            collective_id=1, has_side_effects=True, vmem_limit_bytes=67043328
+            collective_id=1, has_side_effects=True, vmem_limit_bytes=58720256
         ),
     )(*operands)
 
@@ -1220,6 +1408,7 @@
     rows_dev, model_width = resid.shape
     capacity = max(2, 3 * rows_dev // experts)
     fits = capacity % RIM == 0 and rows_dev % LANES == 0
+    fits = fits and gate_weight.shape[2] % LANES == 0 and gate_weight.shape[2] > LANES
     if fits and tp_size == 4 and experts >= 4 and experts & (experts - 1) == 0:
         return fused_layer(
             resid,

time: 132 us -> 111 us (0.84)
  Pallas kernels: 130 us -> 109 us
    pallas_call x1, Pallas kernels: 130 us -> 109 us  [fused_layer(): pl.pallas_call(functools.partial(layer_kernel, sp_size, tp_size, capacity...]
where the time goes in v2:
time: 111 us
  Pallas kernels  109 us (98%)
  local copies, waits for them, and re-layouts  1.88 us (2%)
    pallas_call x1, Pallas kernels, fused_layer(): pl.pallas_call(functools.partial(layer_kernel, sp_size, tp_size, capacity...  109 us

profile of v2, /device:TPU:0, one launch (start us, length us, event | category | flops | bytes accessed | tf_op | source)
XLA Modules:
  0.0 110.7 jit_solution(8335560127901245462)
XLA Ops:
  0.0 108.8 %shard_map.145 = bf16[128,2048]{1,0:T(8,128)(2,1)} custom-call(bf16[512,512]{1,0:T(8,128)(2,1)} %x_hbm.1, bf16[512,512]{1,0:T(8,128)(2,1)} %out_gate_hbm.1, f32[4,512]{1,0:T(4,128)} %taps_hbm.1, bf16[8,64,64]{2,1,0:T(8,128)(2,1)} %recur_map_hbm.1, bf16[8,64,64]{2,1,0:T(8,128)(2,1)} %input_map_hbm.1, f32[1,512]{1,0:T(1,128)} %bitcast.8, ...), custom_call_target="tpu_custom_call" | custom-call | tf_op jit(solution)/shard_map/pallas_call | solution.py:1316
  108.8 1.9 %copy.17 = bf16[128,2048]{1,0:T(8,128)(2,1)} copy(bf16[128,2048]{1,0:T(8,128)(2,1)} %shard_map.145) | data formatting | bytes 1048576

commit v3 on v2

--- a/solution.py
+++ b/solution.py
@@ -749,7 +749,6 @@
 
     with phase("project"):
         project(other, across, 0, True)
-        project(far, along, 1, False)
 
     def far_copy(q):
         return pltpu.make_async_remote_copy(
@@ -770,8 +769,7 @@
                 sum_far = across[core, at, cols] + recv_pair[0, n, at, :].astype(jnp.float32)
                 send_far[at, cols] = sum_far.astype(jnp.bfloat16)
             far_copy(q).start()
-    for n in range(steps):
-        pair_copy(1, n).start()
+    project(far, along, 1, True)
     for n in range(steps):
         cols = slice(n * step, (n + 1) * step)
         pair_copy(1, n).wait_recv()
@@ -1287,7 +1285,7 @@
     hidden, columns = gate_weight.shape[2], down_weight.shape[2]
     step = 512 if width % 512 == 0 else width
     steps = width // step
-    pieces = 4 if rows_dev % (4 * RIM) == 0 else 1
+    pieces = 8 if rows_dev % (8 * RIM) == 0 else 1
     half = sp_size // 2
     slots_all = tp_size * capacity
     narrow = (

time: 111 us -> 110 us (level)
  no operation moved by 1% of the time
where the time goes in v3:
time: 110 us
  Pallas kernels  108 us (98%)
  local copies, waits for them, and re-layouts  1.88 us (2%)
    pallas_call x1, Pallas kernels, fused_layer(): pl.pallas_call(functools.partial(layer_kernel, sp_size, tp_size, capacity...  108 us

profile of v3, /device:TPU:0, one launch (start us, length us, event | category | flops | bytes accessed | tf_op | source)
XLA Modules:
  0.0 110.0 jit_solution(4060984692008984108)
XLA Ops:
  0.0 108.1 %shard_map.145 = bf16[128,2048]{1,0:T(8,128)(2,1)} custom-call(bf16[512,512]{1,0:T(8,128)(2,1)} %x_hbm.1, bf16[512,512]{1,0:T(8,128)(2,1)} %out_gate_hbm.1, f32[4,512]{1,0:T(4,128)} %taps_hbm.1, bf16[8,64,64]{2,1,0:T(8,128)(2,1)} %recur_map_hbm.1, bf16[8,64,64]{2,1,0:T(8,128)(2,1)} %input_map_hbm.1, f32[1,512]{1,0:T(1,128)} %bitcast.8, ...), custom_call_target="tpu_custom_call" | custom-call | tf_op jit(solution)/shard_map/pallas_call | solution.py:1314
  108.1 1.9 %copy.17 = bf16[128,2048]{1,0:T(8,128)(2,1)} copy(bf16[128,2048]{1,0:T(8,128)(2,1)} %shard_map.145) | data formatting | bytes 1048576
